TPU v7x, 256 devices: a whole 4x4x8 slice. The times are simulated.
256 devices in a mesh: fs: 16 (over y, x), tp: 16 (over z, core).
Axes of the slice: x: 4, y: 4, z: 8, core: 2. Of those that a mesh axis runs over, the one named last changes fastest.
Arguments:
- tokens: bfloat16 [2048, 4096], P('fs', 'tp'), may hold values from -6 to 6
- expert_ids: int32 [2048, 8], P('fs'), may hold values from 0 to 63, all different within a row; in each aligned block of 128 rows (0 to 127, 128 to 255, ...) at most 32 rows name the same one
- affinity: float32 [2048, 8], P('fs'), may hold values from 0.05 to 1
- norm_gain: float32 [4096], P('fs'), may hold values from 0.1 to 1.9
- gate_train: float32 [64, 512, 4096], P(None, 'tp', 'fs'), may hold values from -0.09375 to 0.09375
- up_train: float32 [64, 512, 4096], P(None, 'tp', 'fs'), may hold values from -0.09375 to 0.09375
- down_train: float32 [64, 512, 4096], P(None, 'fs', 'tp'), may hold values from -0.25 to 0.25
- shared_gate_train: float32 [512, 4096], P('tp', 'fs'), may hold values from -0.09375 to 0.09375
- shared_up_train: float32 [512, 4096], P('tp', 'fs'), may hold values from -0.09375 to 0.09375
- shared_down_train: float32 [512, 4096], P('fs', 'tp'), may hold values from -0.25 to 0.25
Outputs:
- mixed: bfloat16 [2048, 4096], P('fs', 'tp')
- gate_serve: bfloat16 [64, 512, 4096], P('fs', 'tp')
- up_serve: bfloat16 [64, 512, 4096], P('fs', 'tp')
- down_serve: bfloat16 [64, 512, 4096], P('fs', None, 'tp')
- shared_gate_serve: bfloat16 [512, 4096], P('tp')
- shared_up_serve: bfloat16 [512, 4096], P('tp')
- shared_down_serve: bfloat16 [512, 4096], P(None, 'tp')
Inputs may be any that keep to these rules, and one draw needn't show every extreme that they name: `expert_ids`: each row names 8 different experts. In each aligned block of 128 rows (the tokens of one index of fs) no expert is named by more than 32 rows, a bound that some block reaches.
All inputs are finite; a program needn't handle non-finite values.
Results may differ from a plain program's by a relative error of at most 0.019.
Values may be sent and summed in bfloat16 or wider, within the bound.
A program may use at most 128 MiB of HBM per device.

v0:
```python
import jax
import jax.numpy as jnp
from jax import lax
from jax.sharding import PartitionSpec as P

EXPERTS = 64
K = 8
CAP = 32


norm_eps = 1e-06
routed_scale = 2.5


def side_by_side(arrays, axis, dim, along):
    both = jnp.concatenate(arrays, axis=along)
    filled, at, done = (lax.all_gather(both, axis, axis=dim, tiled=True), 0, [])
    for a in arrays:
        done.append(lax.slice_in_dim(filled, at, at + a.shape[along], axis=along))
        at += a.shape[along]
    return tuple(done)


def side_by_side_2(arrays, axis, split_dim, concat_dim, along):
    widths = [a.shape[along] for a in arrays]
    both = jnp.concatenate(arrays, axis=along)
    filled = lax.all_to_all(both, axis, split_axis=split_dim, concat_axis=concat_dim, tiled=True)
    return tuple(jnp.split(filled, [sum(widths[:k]) for k in range(1, len(widths))], axis=along))


def gather_turned(arrays, axis, dims):
    turned = [jnp.moveaxis(a, dim, 0) for a, dim in zip(arrays, dims)]
    both = jnp.concatenate([t.reshape(len(t), -1) for t in turned], axis=1)
    filled, at, done = (lax.all_gather(both, axis, axis=0, tiled=True), 0, [])
    for t, dim in zip(turned, dims):
        share = filled[:, at : at + t[0].size].reshape(-1, *t.shape[1:])
        done.append(jnp.moveaxis(share, 0, dim))
        at += t[0].size
    return tuple(done)


def body(
    tokens,
    expert_ids,
    affinity,
    norm_gain,
    gate_train,
    up_train,
    down_train,
    shared_gate_train,
    shared_up_train,
    shared_down_train,
):
    gain_cols = norm_gain[None, None, :]
    gate_send = (gate_train * gain_cols).astype(jnp.bfloat16)
    up_send = (up_train * gain_cols).astype(jnp.bfloat16)
    down_send = down_train.astype(jnp.bfloat16)
    shared_gate_serve, shared_up_serve, shared_down_serve = (
        *side_by_side(
            (
                (shared_gate_train * norm_gain[None, :]).astype(jnp.bfloat16),
                (shared_up_train * norm_gain[None, :]).astype(jnp.bfloat16),
            ),
            "fs",
            1,
            0,
        ),
        lax.all_gather(shared_down_train.astype(jnp.bfloat16), "fs", axis=0, tiled=True),
    )
    gate_serve, up_serve = side_by_side_2((gate_send, up_send), "fs", 0, 2, 1)
    full_rows = lax.all_gather(tokens, "tp", axis=1, tiled=True)
    widened = full_rows.astype(jnp.float32)
    inverse_rms = lax.rsqrt(jnp.mean(widened * widened, axis=1) + norm_eps)
    shared_gate = (
        jnp.einsum("td,hd->th", full_rows, shared_gate_serve, preferred_element_type=jnp.float32)
        * inverse_rms[:, None]
    )
    shared_up = (
        jnp.einsum("td,hd->th", full_rows, shared_up_serve, preferred_element_type=jnp.float32)
        * inverse_rms[:, None]
    )
    shared_hidden = (jax.nn.silu(shared_gate) * shared_up).astype(jnp.bfloat16)
    token_count = tokens.shape[0]
    flat_ids = expert_ids.reshape(-1)
    onehot = (flat_ids[:, None] == jnp.arange(EXPERTS, dtype=jnp.int32)[None, :]).astype(jnp.int32)
    slot_index = jnp.sum((jnp.cumsum(onehot, axis=0) - onehot) * onehot, axis=1)
    position = flat_ids * CAP + slot_index
    token_of = jnp.repeat(jnp.arange(token_count, dtype=jnp.int32), K)
    row_scale = (
        jnp.zeros((EXPERTS * CAP,), jnp.float32)
        .at[position]
        .set(inverse_rms[token_of])
        .reshape(EXPERTS, CAP)
    )
    outgoing = (
        jnp.zeros((EXPERTS * CAP, tokens.shape[1]), jnp.bfloat16).at[position].set(tokens[token_of])
    )
    strips, arrived_scale = (
        lax.all_to_all(
            outgoing.reshape(EXPERTS, CAP, -1), "fs", split_axis=0, concat_axis=1, tiled=True
        ),
        lax.all_to_all(
            row_scale.astype(jnp.bfloat16), "fs", split_axis=0, concat_axis=1, tiled=True
        ).astype(row_scale.dtype),
    )
    piece = lax.all_gather(strips, "tp", axis=2, tiled=True)
    gate_pre = jnp.einsum("erd,ehd->erh", piece, gate_serve, preferred_element_type=jnp.float32)
    up_pre = jnp.einsum("erd,ehd->erh", piece, up_serve, preferred_element_type=jnp.float32)
    routed_hidden = (
        jax.nn.silu(gate_pre * arrived_scale[:, :, None]) * (up_pre * arrived_scale[:, :, None])
    ).astype(jnp.bfloat16)
    down_serve = lax.all_to_all(down_send, "fs", split_axis=0, concat_axis=1, tiled=True)
    pieces = gather_turned((shared_hidden[None], routed_hidden), "tp", (2, 2))
    shared_out = jnp.einsum(
        "brh,hd->brd", pieces[0], shared_down_serve, preferred_element_type=jnp.float32
    )
    routed_out = jnp.einsum(
        "erh,ehd->erd", pieces[1], down_serve, preferred_element_type=jnp.float32
    )
    returned = lax.all_to_all(
        routed_out.astype(jnp.bfloat16), "fs", split_axis=1, concat_axis=0, tiled=True
    )
    picked = (
        returned.reshape(EXPERTS * CAP, -1)[position]
        .reshape(token_count, K, -1)
        .astype(jnp.float32)
    )
    route_weight = routed_scale * affinity / jnp.sum(affinity, axis=1, keepdims=True)
    routed = jnp.sum(picked * route_weight[:, :, None], axis=1)
    mixed_out = (shared_out[0] + routed).astype(jnp.bfloat16)
    return (
        mixed_out,
        gate_serve,
        up_serve,
        down_serve,
        shared_gate_serve,
        shared_up_serve,
        shared_down_serve,
    )


def solution(mesh):
    return jax.shard_map(
        body,
        mesh=mesh,
        in_specs=(
            P("fs", "tp"),
            P("fs", None),
            P("fs", None),
            P("fs"),
            P(None, "tp", "fs"),
            P(None, "tp", "fs"),
            P(None, "fs", "tp"),
            P("tp", "fs"),
            P("tp", "fs"),
            P("fs", "tp"),
        ),
        out_specs=(
            P("fs", "tp"),
            P("fs", "tp", None),
            P("fs", "tp", None),
            P("fs", None, "tp"),
            P("tp", None),
            P("tp", None),
            P(None, "tp"),
        ),
        check_vma=False,
    )
```

profile of v0, /device:TPU:42, one launch (start us, length us, event | category | flops | bytes accessed | tf_op | source)
XLA Modules:
  0.0 279.9 jit_solution(18277624888805937464)
XLA Ops:
  9.8 18.0 %reduce-window.6 = s32[64,8,128]{2,1,0:T(8,128)S(1)} reduce-window(s32[64,8,128]{2,1,0:T(8,128)S(1)} %fusion.18, s32[]{:T(128)} %constant.8.clone.1), window={size=1x1x128 pad=0_0x0_0x127_0}, to_apply=%region_1.2 | reduce-window | flops 8323072 | bytes 524292 | tf_op jit(solution)/shard_map/reduce-window
  28.6 12.2 %scatter_custom_fusion = bf16[2048,256]{1,0:T(8,128)(2,1)S(1)} fusion(s32[1024]{0:T(1024)S(1)} %bitcast.110, bf16[128,256]{1,0:T(8,128)(2,1)} %param.10, s32[1024]{0:T(1024)S(1)} %broadcast_clamp_fusion.1, bf16[]{:T(256)} %constant.7.clone.1), kind=kCustom, calls=%fused_computation.29 | custom fusion | bytes 1049088 | tf_op jit(solution)/shard_map/scatter | solution.py:96
  40.8 20.8 %all_to_all.79 = bf16[64,32,256]{2,1,0:T(8,128)(2,1)S(1)} all-to-all(bf16[64,32,256]{2,1,0:T(8,128)(2,1)S(1)} %bitcast.100), channel_id=1, replica_groups=mesh['fs'=16,'tp'=16] {'fs'}, dimensions={0} | all-to-all | bytes 2097152 | tf_op jit(solution)/shard_map/all_to_all | solution.py:99
  63.6 2.2 multiply_convert_fusion.1
  67.3 7.2 %all-to-all-start.1 = ((bf16[64,64,256]{2,1,0:T(8,128)(2,1)}), bf16[64,64,256]{2,1,0:T(8,128)(2,1)S(1)}, u32[]{:S(2)}, u32[]{:S(2)}) async-start(bf16[64,64,256]{2,1,0:T(8,128)(2,1)} %pad_maximum_fusion), calls=%async_computation.1 | async-start | bytes 4194304 | tf_op jit(solution)/shard_map/all_to_all | solution.py:27
  74.6 41.6 %all_gather.15 = bf16[64,4096]{1,0:T(8,128)(2,1)S(1)} all-gather(bf16[64,256]{1,0:T(8,128)(2,1)S(1)} %pad_maximum_fusion.2), channel_id=1, replica_groups=mesh['fs'=16,'tp'=16] {'fs'}, dimensions={1}, use_global_device_ids=true | all-gather | bytes 557056 | tf_op jit(solution)/shard_map/all_gather | solution.py:17
  116.9 2.5 copy.65
  119.4 2.9 %all_to_all.65 = bf16[4,64,4096]{2,1,0:T(8,128)(2,1)S(1)} reshape(bf16[4,64,16,256]{3,2,1,0:T(8,128)(2,1)} %bitcast.97) | data formatting | bytes 4194304 | tf_op jit(solution)/shard_map/all_to_all | solution.py:27
  123.9 6.6 %gather_fusion = f32[1024]{0:T(1024)S(1)} fusion(f32[128]{0:T(128)S(1)} %add_rsqrt_fusion, s32[1024]{0:T(1024)S(1)} %broadcast_clamp_fusion.1), kind=kCustom, calls=%fused_computation.1 | custom fusion | bytes 12288 | tf_op jit(solution)/shard_map/gather | solution.py:92
  130.5 4.3 %scatter_custom_fusion.1 = f32[2048]{0:T(1024)S(1)} fusion(s32[1024]{0:T(1024)S(1)} %bitcast.111, f32[1024]{0:T(1024)S(1)} %gather_fusion, f32[]{:T(128)} %constant.10.clone.1), kind=kCustom, calls=%fused_computation.49 | custom fusion | bytes 8196 | tf_op jit(solution)/shard_map/scatter | solution.py:92
  135.5 6.7 %all-to-all-start.2 = ((bf16[16,4,32]{2,1,0:T(4,128)(2,1)}), bf16[16,4,32]{2,1,0:T(4,128)(2,1)S(1)}, u32[]{:S(2)}, u32[]{:S(2)}) async-start(bf16[16,4,32]{2,1,0:T(4,128)(2,1)} %convert_element_type.76), calls=%async_computation.2 | async-start | bytes 32768 | tf_op jit(solution)/shard_map/all_to_all | solution.py:102
  144.9 2.7 all-to-all-done.2
  147.6 18.2 %all-gather.6.cloned.1.call-done = bf16[4,512,4096]{2,1,0:T(8,128)(2,1)} async-done(((bf16[4,512,256]{2,1,0:T(8,128)(2,1)}), bf16[4,512,4096]{2,1,0:T(8,128)(2,1)}) %all-gather.6.cloned.1.call-update) | async-done | bytes 16777232 | tf_op jit(solution)/shard_map/all_gather | solution.py:106
  165.8 10.5 %fusion = f32[32,4,512]{2,0,1:T(8,128)S(1)} fusion(bf16[4,512,4096]{2,1,0:T(8,128)(2,1)} %all-gather.6.cloned.1.call-done, bf16[4,32,4096]{2,1,0:T(8,128)(2,1)S(1)} %copy-done.3, f32[4,512]{1,0:T(4,128)S(1)} %reshape.151), kind=kOutput, calls=%fused_computation.13 | convolution fusion | flops 536936448 | bytes 18096128 | tf_op jit(solution)/shard_map/erd,ehd->erh/dot_general | solution.py:107
  176.6 5.1 %fusion.4 = bf16[4,4,8,512]{3,2,1,0:T(8,128)(2,1)S(1)} fusion(bf16[4,512,4096]{2,1,0:T(8,128)(2,1)S(1)} %copy-done, bf16[4,32,4096]{2,1,0:T(8,128)(2,1)S(1)} %copy-done.4, f32[32,4,512]{2,0,1:T(8,128)S(1)} %fusion, f32[4,512]{1,0:T(4,128)S(1)} %reshape.151), kind=kOutput, calls=%fused_computation.17 | convolution fusion | flops 537329664 | bytes 18227200 | tf_op jit(solution)/shard_map/erd,ehd->erh/dot_general | solution.py:108
  182.4 1.7 convert_element_type.82
  184.2 21.2 %all_to_all.80 = bf16[64,32,256]{2,1,0:T(8,128)(2,1)S(1)} all-to-all(bf16[64,32,256]{2,1,0:T(8,128)(2,1)S(1)} %convert_element_type.82), channel_id=1, replica_groups=mesh['fs'=16,'tp'=16] {'fs'}, dimensions={0} | all-to-all | bytes 2097152 | tf_op jit(solution)/shard_map/all_to_all | solution.py:112
  205.5 14.9 %all-gather.8.cloned.1.call-done = bf16[512,2176]{1,0:T(8,128)(2,1)} async-done(((bf16[32,2176]{1,0:T(8,128)(2,1)}), bf16[512,2176]{1,0:T(8,128)(2,1)}) %all-gather.8.cloned.1.call-update) | async-done | bytes 2228240 | tf_op jit(solution)/shard_map/all_gather | solution.py:34
  221.9 2.5 copy.56
  224.4 2.3 convolution_convert_fusion
  226.7 1.8 copy.58
  228.5 7.1 %all-to-all-start.4 = ((bf16[4,512,256]{2,0,1:T(4,128)(2,1)}), bf16[4,512,256]{2,0,1:T(4,128)(2,1)S(1)}, u32[]{:S(2)}, u32[]{:S(2)}) async-start(bf16[4,512,256]{2,0,1:T(4,128)(2,1)} %copy.58), calls=%async_computation.4 | async-start | bytes 2097152 | tf_op jit(solution)/shard_map/all_to_all | solution.py:120
  236.4 28.7 %all_gather.19 = bf16[512,256]{1,0:T(8,128)(2,1)S(1)} all-gather(bf16[32,256]{1,0:T(8,128)(2,1)S(1)} %convert_element_type.81), channel_id=1, replica_groups=mesh['fs'=16,'tp'=16] {'fs'}, dimensions={0}, use_global_device_ids=true | all-gather | bytes 278528 | tf_op jit(solution)/shard_map/all_gather | solution.py:68
  265.4 4.9 %gather_fusion.1 = bf16[1024,256]{1,0:T(8,128)(2,1)} fusion(bf16[2048,256]{1,0:T(8,128)(2,1)S(1)} %bitcast.95, s32[1024]{0:T(1024)S(1)} %broadcast_clamp_fusion), kind=kCustom, calls=%fused_computation.2 | custom fusion | bytes 1052672 | tf_op jit(solution)/shard_map/gather | solution.py:124
  (85 shorter events, 19.2 us)
Async XLA Ops:
  7.2 115.2 %all-gather.4.cloned.1.call-start = ((), (), s32[]{:S(2)}) async-start(), calls=%async_computation.5 | async-start | bytes 1114112 | tf_op jit(solution)/shard_map/all_gather | solution.py:71
  7.9 157.9 %all-gather.6.cloned.1.call-start = ((), (), s32[]{:S(2)}) async-start(), calls=%async_computation.6 | async-start | bytes 17825792 | tf_op jit(solution)/shard_map/all_gather | solution.py:106
  61.6 2.0 copy-start.5
  61.7 2.0 copy-start.13
  67.3 7.2 %copy-start.9 = (f32[32,256]{1,0:T(8,128)S(1)}, f32[32,256]{1,0:T(8,128)}, u32[]{:S(2)}) copy-start(f32[32,256]{1,0:T(8,128)} %param.17) | copy-start | bytes 98308
  67.3 7.3 %copy-start.10 = (f32[32,256]{1,0:T(8,128)S(1)}, f32[32,256]{1,0:T(8,128)}, u32[]{:S(2)}) copy-start(f32[32,256]{1,0:T(8,128)} %param.18) | copy-start | bytes 98308
  67.3 49.6 %all-to-all-start.1 = ((bf16[64,64,256]{2,1,0:T(8,128)(2,1)}), bf16[64,64,256]{2,1,0:T(8,128)(2,1)S(1)}, u32[]{:S(2)}, u32[]{:S(2)}) async-start(bf16[64,64,256]{2,1,0:T(8,128)(2,1)} %pad_maximum_fusion), calls=%async_computation.1 | async-start | bytes 4194304 | tf_op jit(solution)/shard_map/all_to_all | solution.py:27
  116.9 25.6 %copy-start.7 = (bf16[32,4096]{1,0:T(8,128)(2,1)}, bf16[32,4096]{1,0:T(8,128)(2,1)S(1)}, u32[]{:S(2)}) copy-start(bf16[32,4096]{1,0:T(8,128)(2,1)S(1)} %get-tuple-element.26) | copy-start | bytes 786436
  123.9 18.6 %copy-start.1 = (bf16[128,4096]{1,0:T(8,128)(2,1)S(1)}, bf16[128,4096]{1,0:T(8,128)(2,1)}, u32[]{:S(2)}) copy-start(bf16[128,4096]{1,0:T(8,128)(2,1)} %all-gather.4.cloned.1.call-done) | copy-start | bytes 3145732
  135.5 12.1 %all-to-all-start.2 = ((bf16[16,4,32]{2,1,0:T(4,128)(2,1)}), bf16[16,4,32]{2,1,0:T(4,128)(2,1)S(1)}, u32[]{:S(2)}, u32[]{:S(2)}) async-start(bf16[16,4,32]{2,1,0:T(4,128)(2,1)} %convert_element_type.76), calls=%async_computation.2 | async-start | bytes 32768 | tf_op jit(solution)/shard_map/all_to_all | solution.py:102
  142.2 78.1 %all-gather.8.cloned.1.call-start = ((), (), s32[]{:S(2)}) async-start(), calls=%async_computation.7 | async-start | bytes 2367488 | tf_op jit(solution)/shard_map/all_gather | solution.py:34
  142.9 1.5 copy-start.8
  144.4 21.4 %copy-start.3 = (bf16[4,32,4096]{2,1,0:T(8,128)(2,1)S(1)}, bf16[4,32,4096]{2,1,0:T(8,128)(2,1)}, u32[]{:S(2)}) copy-start(bf16[4,32,4096]{2,1,0:T(8,128)(2,1)} %get-tuple-element.23) | copy-start | bytes 3145732
  165.8 10.5 %copy-start = (bf16[4,512,4096]{2,1,0:T(8,128)(2,1)S(1)}, bf16[4,512,4096]{2,1,0:T(8,128)(2,1)}, u32[]{:S(2)}) copy-start(bf16[4,512,4096]{2,1,0:T(8,128)(2,1)} %all-gather.6.cloned.1.call-done) | copy-start | bytes 50331652
  165.8 10.8 %copy-start.4 = (bf16[4,32,4096]{2,1,0:T(8,128)(2,1)S(1)}, bf16[4,32,4096]{2,1,0:T(8,128)(2,1)}, u32[]{:S(2)}) copy-start(bf16[4,32,4096]{2,1,0:T(8,128)(2,1)} %get-tuple-element.24) | copy-start | bytes 3145732
  205.4 19.0 %copy-start.6 = (bf16[16,4,32,256]{3,2,0,1:T(8,128)(2,1)}, bf16[16,4,32,256]{3,2,0,1:T(8,128)(2,1)S(1)}, u32[]{:S(2)}) copy-start(bf16[16,4,32,256]{3,2,0,1:T(8,128)(2,1)S(1)} %copy.57) | copy-start | bytes 3145732
  220.3 1.6 slice-start
  226.7 8.9 %copy-start.12 = (f32[128,8]{0,1:T(8,128)S(1)}, f32[128,8]{0,1:T(8,128)}, u32[]{:S(2)}) copy-start(f32[128,8]{0,1:T(8,128)} %param.12) | copy-start | bytes 12292
  226.7 9.7 %copy-start.11 = (f32[32,256]{1,0:T(8,128)S(1)}, f32[32,256]{1,0:T(8,128)}, u32[]{:S(2)}) copy-start(f32[32,256]{1,0:T(8,128)} %param.19) | copy-start | bytes 98308
  228.5 36.6 %all-to-all-start.4 = ((bf16[4,512,256]{2,0,1:T(4,128)(2,1)}), bf16[4,512,256]{2,0,1:T(4,128)(2,1)S(1)}, u32[]{:S(2)}, u32[]{:S(2)}) async-start(bf16[4,512,256]{2,0,1:T(4,128)(2,1)} %copy.58), calls=%async_computation.4 | async-start | bytes 2097152 | tf_op jit(solution)/shard_map/all_to_all | solution.py:120
  265.4 6.4 %copy-start.2 = (bf16[512,2176]{1,0:T(8,128)(2,1)S(1)}, bf16[512,2176]{1,0:T(8,128)(2,1)}, u32[]{:S(2)}) copy-start(bf16[512,2176]{1,0:T(8,128)(2,1)} %all-gather.8.cloned.1.call-done) | copy-start | bytes 6684676
Sparse Core Ops, SparseCore 0:
  9.7 39.7 all-gather.3
  62.9 102.9 all-gather.5
  182.5 37.7 all-gather.7
where the time goes:
time: 283 us; the launch traced here: 280 us
  blocking collectives  112 us (40%)
  local copies, waits for them, and re-layouts  47.9 us (17%)
  waiting for transfers between devices  36.5 us (13%)
  other arithmetic  28.1 us (10%)
  starting transfers between devices  21.4 us (8%)
  matrix products  19.6 us (7%)
  between operations  14.1 us (5%)
    all_gather x1, blocking collectives, side_by_side(): filled, at, done = (lax.all_gather(both, axis, axis=dim, tiled=True), 0, [])  41.6 us
    all_gather x1, blocking collectives, body(): lax.all_gather(shared_down_train.astype(jnp.bfloat16), 'fs', axis=0, tile...  28.7 us
    all_to_all x1, blocking collectives, body(): lax.all_to_all(down_send, 'fs', split_axis=0, concat_axis=1, tiled=True)  21.2 us
    all_to_all x1, blocking collectives, body(): lax.all_to_all(outgoing.reshape(EXPERTS, CAP, -1), 'fs', split_axis=0, co...  20.8 us
    another operation x3, other arithmetic  18.2 us
    all_gather x1, waiting for transfers between devices, body(): piece = lax.all_gather(strips, 'tp', axis=2, tiled=True)  18.2 us
    all_gather x1, waiting for transfers between devices, gather_turned(): filled, at, done = (lax.all_gather(both, axis, axis=0, tiled=True), 0, [])  14.9 us
    scatter x1, local copies, waits for them, and re-layouts, body(): jnp.zeros((EXPERTS * CAP, tokens.shape[1]), jnp.bfloat16).at[position]  12.2 us
  transfers between devices with their start and end apart: 6, of which 3 were waited for; matrix products, arithmetic and copies ran while one was open for 21% of the time, Pallas kernels for 0%

commit v1 on v0

v1 whole, which is shorter than its diff:
```python
import functools

import jax
import jax.numpy as jnp
from jax import lax
from jax.experimental import pallas as pl
from jax.experimental.pallas import tpu as pltpu
from jax.sharding import PartitionSpec as P

K = 8
NORM_EPS = 1e-06
ROUTED_SCALE = 2.5
LANES = 128
F32 = jnp.float32
BF16 = jnp.bfloat16
NT_DIMS = (((1,), (1,)), ((), ()))
TN_DIMS = (((0,), (0,)), ((), ()))


def silu(v):
    return v / (1.0 + jnp.exp(-v))


def kernel(
    NF,
    NT,
    D,
    tok_ref,
    ids_ref,
    aff_ref,
    gain_ref,
    gt_ref,
    ut_ref,
    dt_ref,
    sgt_ref,
    sut_ref,
    sdt_ref,
    mixed_ref,
    gs_ref,
    us_ref,
    ds_ref,
    sgs_ref,
    sus_ref,
    sds_ref,
    wf,
    wg,
    wu,
    wd,
    ws,
    fold,
    spread_ids,
    wexp,
    idt,
    xz,
    xa,
    hv,
    hz,
    ha,
    dk,
    gsc,
    usc,
    tsc,
    asc,
    psend,
    precv,
    osend,
    orecv,
    load_sem,
    own_sem,
    ids_s,
    ids_r,
    xzs,
    xzr,
    xps,
    xpr,
    xms,
    xmr,
    hzs,
    hzr,
    hps,
    hpr,
    hms,
    hmr,
    p_s,
    p_r,
    o_s,
    o_r,
    w_s,
    w_r,
):
    f = lax.axis_index("fs")
    t = lax.axis_index("tp")
    z, c = t // 2, t % 2
    NZ = NT // 2
    TOK, DS = tok_ref.shape
    HS = sgt_ref.shape[0]
    EH = wg.shape[0]
    EP = EH // HS // NF
    GROUPS = EH // LANES
    ROWS = EP * HS

    loads = []
    for i, r in enumerate((gt_ref, ut_ref, dt_ref)):
        load = pltpu.make_async_copy(r, wf.at[i], load_sem.at[i])
        load.start()
        loads.append(load)

    bar = pltpu.get_barrier_semaphore()

    def greet_plane(i, carry):
        at = (f * 2 + c + i) % (2 * NF)
        pl.semaphore_signal(
            bar, 1, device_id={"fs": at // 2, "tp": z * 2 + at % 2},
            device_id_type=pl.DeviceIdType.MESH,
        )
        return carry

    def greet_column(i, carry):
        pl.semaphore_signal(
            bar, 1, device_id={"tp": ((z + i) % NZ) * 2 + c},
            device_id_type=pl.DeviceIdType.MESH,
        )
        return carry

    lax.fori_loop(1, 2 * NF, greet_plane, 0)
    lax.fori_loop(1, NZ, greet_column, 0)

    eye = (
        lax.broadcasted_iota(jnp.int32, (TOK, TOK), 0)
        == lax.broadcasted_iota(jnp.int32, (TOK, TOK), 1)
    ).astype(BF16)
    ids16 = jnp.concatenate([ids_ref[...].astype(F32).astype(BF16), jnp.zeros((TOK, 8), BF16)], axis=1)
    idt[f] = lax.dot_general(ids16, eye, TN_DIMS, preferred_element_type=F32).astype(BF16)

    pl.semaphore_wait(bar, 2 * NF - 1 + NZ - 1)

    def remote(src, dst, s, r, **where):
        return pltpu.make_async_remote_copy(
            src_ref=src, dst_ref=dst, send_sem=s, recv_sem=r,
            device_id=where, device_id_type=pl.DeviceIdType.MESH,
        )

    steps = [i for d in range(1, NZ // 2 + 1) for i in dict.fromkeys((d, NZ - d))]

    def along_z(src, stage, s, r):
        for i in steps:
            remote(src, stage.at[z], s.at[i], r.at[z], tp=((z + i) % NZ) * 2 + c).start()

    def in_plane(src, stage, got, zs, zr, s, r):
        for i in [0] + [(NZ - i) for i in steps]:
            zz = (z + i) % NZ
            if i:
                remote(src, stage.at[zz], zs.at[i], zr.at[zz], tp=zz * 2 + c).wait_recv()
            part = stage.at[zz] if i else src
            to = zz * 2 + c

            @pl.when(to == f)
            def _():
                got[f] = part[...]

            @pl.when(to != f)
            def _():
                remote(part, got.at[f], s.at[i], r.at[f], fs=to, tp=z * 2 + f % 2).start()

    def wait_spread_sends(src, stage, got, zs, zr, s, r):
        for i in range(NZ):
            zz = (z + i) % NZ
            to = zz * 2 + c
            if i:
                remote(src, stage.at[z], zs.at[i], zr.at[z], tp=zz * 2 + c).wait_send()

            @pl.when(to != f)
            def _():
                remote(src, got.at[f], s.at[i], r.at[f], fs=to, tp=z * 2 + f % 2).wait_send()

    def direct_block(i):
        return 2 * ((f // 2 + i) % (NF // 2)) + c

    def mate_block(i):
        return 2 * ((f // 2 + i) % (NF // 2)) + 1 - c

    def take_direct(b, got, s, r, ms, mr):
        @pl.when(b != f)
        def _():
            remote(got.at[b], got.at[b], s.at[0], r.at[b], fs=b).wait_recv()

        remote(got.at[b], got.at[b], ms.at[b], mr.at[b], tp=z * 2 + 1 - c).start()

    def take_mate(b, got, ms, mr):
        remote(got.at[b], got.at[b], ms.at[b], mr.at[b], tp=z * 2 + 1 - c).wait_recv()

    def wait_mate_sends(got, ms, mr):
        def body(i, carry):
            b = direct_block(i)
            remote(got.at[b], got.at[b], ms.at[b], mr.at[b], tp=z * 2 + 1 - c).wait_send()
            return carry

        lax.fori_loop(0, NF // 2, body, 0)

    along_z(tok_ref, xz, xzs, xzr)

    def send_ids(i, carry):
        remote(idt.at[f], idt.at[f], ids_s.at[i], ids_r.at[f], fs=(f + i) % NF).start()
        return carry

    lax.fori_loop(1, NF, send_ids, 0)

    fr = lax.broadcasted_iota(jnp.int32, (4 * LANES, LANES), 0)
    fc = lax.broadcasted_iota(jnp.int32, (4 * LANES, LANES), 1)
    fold[...] = ((fr // LANES == fc // HS) & (fr % HS == fc % HS)).astype(BF16)
    sr = lax.broadcasted_iota(jnp.int32, (16, K * LANES), 0)
    sc = lax.broadcasted_iota(jnp.int32, (16, K * LANES), 1)
    spread_ids[...] = (sr == sc // LANES).astype(BF16)

    affinity = aff_ref[...]
    weight = ROUTED_SCALE * affinity / jnp.sum(affinity, axis=1, keepdims=True)
    wr = lax.broadcasted_iota(jnp.int32, (K, K * HS), 0)
    wc = lax.broadcasted_iota(jnp.int32, (K, K * HS), 1)
    place = (wr == wc // HS).astype(BF16)
    high = weight.astype(BF16)
    rest = weight - high.astype(F32)
    middle = rest.astype(BF16)
    low = (rest - middle.astype(F32)).astype(BF16)
    wexp[...] = (
        jnp.dot(high, place, preferred_element_type=F32)
        + jnp.dot(middle, place, preferred_element_type=F32)
        + jnp.dot(low, place, preferred_element_type=F32)
    )

    gain = gain_ref[...]
    ws[...] = jnp.zeros_like(ws)
    ws[0:HS, :] = (sgt_ref[...] * gain).astype(BF16)
    ws[HS : 2 * HS, :] = (sut_ref[...] * gain).astype(BF16)
    loads[0].wait()
    loads[1].wait()

    def convert_gate_up(i, carry):
        rows = pl.ds(pl.multiple_of(i * ROWS, ROWS), ROWS)
        wg[rows, :] = (wf[0, rows, :] * gain).astype(BF16)
        wu[rows, :] = (wf[1, rows, :] * gain).astype(BF16)
        return carry

    lax.fori_loop(0, NF, convert_gate_up, 0)

    in_plane(tok_ref, xz, xa, xzs, xzr, xps, xpr)

    wd[EP * NF : EP * NF + EP] = jnp.zeros((EP, HS, DS), BF16)
    wd[EP * NF] = sdt_ref[...].astype(BF16)
    loads[2].wait()

    def convert_down(i, carry):
        rows = pl.ds(pl.multiple_of(i * ROWS, ROWS), ROWS)
        wd[pl.ds(i * EP, EP)] = wf[2, rows, :].reshape(EP, HS, DS).astype(BF16)
        return carry

    lax.fori_loop(0, NF, convert_down, 0)

    def pieces(j, src_of):
        cols = pl.ds(pl.multiple_of(src_of * DS, DS), DS)
        rows = pl.ds(pl.multiple_of(j * ROWS, ROWS), ROWS)
        hid = pl.ds(pl.multiple_of(src_of * HS, HS), HS)
        return (
            (wg.at[rows, :], gs_ref.at[:, cols]),
            (wu.at[rows, :], us_ref.at[:, cols]),
            (wd.at[pl.ds(j * EP, EP)], ds_ref.at[:, hid, :]),
            (ws.at[0:HS, :], sgs_ref.at[:, cols]),
            (ws.at[HS : 2 * HS, :], sus_ref.at[:, cols]),
            (wd.at[EP * NF], sds_ref.at[hid, :]),
        )

    def send_weights(i, which):
        j = (f + i) % NF
        for n, (src, dst) in enumerate(pieces(j, f)):
            if n in which:
                remote(src, dst, w_s.at[n, i], w_r.at[n, f], fs=j).start()

    for n, (src, dst) in enumerate(pieces(f, f)):
        pltpu.make_async_copy(src, dst, own_sem.at[n]).start()

    def partial(b):
        x = xa[b]
        step = 4 * LANES
        for n in range(EH // step):
            part = slice(n * step, (n + 1) * step)
            gsc[:, part] = lax.dot_general(
                x, wg[part, :], NT_DIMS, preferred_element_type=F32
            ).astype(BF16)
            usc[:, part] = lax.dot_general(
                x, wu[part, :], NT_DIMS, preferred_element_type=F32
            ).astype(BF16)
        lane = lax.broadcasted_iota(jnp.int32, (TOK, K * LANES), 1)
        ids = lax.dot_general(idt[b], spread_ids[...], TN_DIMS, preferred_element_type=F32)
        dk[b] = (ids - ((lane % LANES) // HS).astype(F32)).astype(BF16)

        def select(r, carry):
            rows = pl.ds(pl.multiple_of(r * 16, 16), 16)
            at = [dk[b, rows, k * LANES : (k + 1) * LANES] for k in range(K)]
            gate = [jnp.zeros((16, LANES), BF16)] * K
            up = [jnp.zeros((16, LANES), BF16)] * K
            for g in range(GROUPS):
                gv = gsc[rows, g * LANES : (g + 1) * LANES]
                uv = usc[rows, g * LANES : (g + 1) * LANES]
                for k in range(K):
                    hit = at[k] == jnp.asarray(LANES // HS * g, BF16)
                    gate[k] = jnp.where(hit, gv, gate[k])
                    up[k] = jnp.where(hit, uv, up[k])
            for k in range(K):
                tsc[0, rows, k * LANES : (k + 1) * LANES] = gate[k]
                tsc[1, rows, k * LANES : (k + 1) * LANES] = up[k]
            return carry

        lax.fori_loop(0, TOK // 16, select, 0)
        for n in range(2):
            for j in range(2):
                at = (2 * n + j) * LANES
                psend[b, :, at : at + LANES] = jnp.dot(
                    tsc[n, :, j * 4 * LANES : (j + 1) * 4 * LANES],
                    fold[...],
                    preferred_element_type=F32,
                ).astype(BF16)
        shared = lax.dot_general(x, ws[...], NT_DIMS, preferred_element_type=F32)
        xf = x.astype(F32)
        square = jnp.sum(xf * xf, axis=1, keepdims=True)
        first = square.astype(BF16).astype(F32)
        lane = lax.broadcasted_iota(jnp.int32, (TOK, LANES), 1)
        tail = jnp.where(lane < 2 * HS, shared, jnp.where(lane < 3 * HS, first, square - first))
        psend[b, :, 4 * LANES : 5 * LANES] = tail.astype(BF16)

    def send_partial(b):
        @pl.when(b != f)
        def _():
            remote(psend.at[b], precv.at[f], p_s.at[b], p_r.at[f], fs=b).start()

    def take_ids(b):
        @pl.when(b != f)
        def _():
            remote(idt.at[b], idt.at[b], ids_s.at[0], ids_r.at[b], fs=b).wait_recv()

    def first_half(i, carry):
        b = direct_block(i)
        take_ids(b)
        take_direct(b, xa, xps, xpr, xms, xmr)
        partial(b)
        send_partial(b)

        @pl.when(i > 0)
        def _():
            send_weights(i, (0, 1, 2, 3, 4, 5))

        return carry

    lax.fori_loop(0, NF // 2, first_half, 0)

    def second_half(i, carry):
        b = mate_block(i)
        take_ids(b)
        take_mate(b, xa, xms, xmr)
        partial(b)
        send_partial(b)
        return carry

    lax.fori_loop(0, NF // 2, second_half, 0)

    def rest_weights(i, carry):
        send_weights(i, (0, 1, 2, 3, 4, 5))
        return carry

    lax.fori_loop(NF // 2, NF, rest_weights, 0)

    def take_partial(i, carry):
        j = (f + i) % NF
        remote(psend.at[j], precv.at[j], p_s.at[j], p_r.at[j], fs=j).wait_recv()
        return carry

    lax.fori_loop(1, NF, take_partial, 0)

    def finish_hidden(r, carry):
        rows = pl.ds(pl.multiple_of(r * 16, 16), 16)
        total = psend[f, rows, :].astype(F32)
        for i in range(1, NF):
            total = total + precv[(f + i) % NF, rows, :].astype(F32)
        at = 4 * LANES + 2 * HS
        square = total[:, at : at + 1] + total[:, at + HS : at + HS + 1]
        inverse_rms = lax.rsqrt(square * (1.0 / D) + NORM_EPS)
        half = K * HS
        gate = total[:, :half] * inverse_rms
        up = total[:, half : 2 * half] * inverse_rms
        hv[rows, :half] = (silu(gate) * up * wexp[rows, :]).astype(BF16)
        tail = total[:, 4 * LANES :] * inverse_rms
        lane = lax.broadcasted_iota(jnp.int32, (16, LANES), 1)
        shared = silu(tail) * pltpu.roll(tail, LANES - HS, 1)
        hv[rows, half : half + LANES] = jnp.where(lane < HS, shared, 0.0).astype(BF16)
        return carry

    lax.fori_loop(0, TOK // 16, finish_hidden, 0)

    along_z(hv, hz, hzs, hzr)
    in_plane(hv, hz, ha, hzs, hzr, hps, hpr)

    def down(b):
        for j in range(2):
            tsc[0, :, j * 4 * LANES : (j + 1) * 4 * LANES] = lax.dot_general(
                ha[b, :, j * LANES : (j + 1) * LANES],
                fold[...],
                NT_DIMS,
                preferred_element_type=F32,
            ).astype(BF16)

        def scatter(r, carry):
            rows = pl.ds(pl.multiple_of(r * 16, 16), 16)
            at = [dk[b, rows, k * LANES : (k + 1) * LANES] for k in range(K)]
            hid = [tsc[0, rows, k * LANES : (k + 1) * LANES] for k in range(K)]
            for g in range(GROUPS):
                a = jnp.zeros((16, LANES), BF16)
                for k in range(K):
                    a = jnp.where(at[k] == jnp.asarray(LANES // HS * g, BF16), hid[k], a)
                asc[rows, g * LANES : (g + 1) * LANES] = a
            asc[rows, EH : EH + LANES] = ha[b, rows, 2 * LANES : 3 * LANES]
            return carry

        lax.fori_loop(0, TOK // 16, scatter, 0)
        osend[b] = jnp.dot(
            asc[...], wd[...].reshape(EH + LANES, DS), preferred_element_type=F32
        ).astype(BF16)

    def send_out(b):
        @pl.when(b != f)
        def _():
            remote(osend.at[b], orecv.at[f], o_s.at[b], o_r.at[f], fs=b).start()

    def down_first(i, carry):
        b = direct_block(i)
        take_direct(b, ha, hps, hpr, hms, hmr)
        down(b)
        send_out(b)
        return carry

    def down_second(i, carry):
        b = mate_block(i)
        take_mate(b, ha, hms, hmr)
        down(b)
        send_out(b)
        return carry

    lax.fori_loop(0, NF // 2, down_first, 0)
    lax.fori_loop(0, NF // 2, down_second, 0)

    def take_out(i, carry):
        j = (f + i) % NF
        remote(osend.at[j], orecv.at[j], o_s.at[j], o_r.at[j], fs=j).wait_recv()
        return carry

    lax.fori_loop(1, NF, take_out, 0)

    def finish(r, carry):
        rows = pl.ds(pl.multiple_of(r * 16, 16), 16)
        total = osend[f, rows, :].astype(F32)
        for i in range(1, NF):
            total = total + orecv[(f + i) % NF, rows, :].astype(F32)
        mixed_ref[rows, :] = total.astype(BF16)
        return carry

    lax.fori_loop(0, TOK // 16, finish, 0)

    for n, (src, dst) in enumerate(pieces(f, f)):
        pltpu.make_async_copy(src, dst, own_sem.at[n]).wait()
    wait_spread_sends(tok_ref, xz, xa, xzs, xzr, xps, xpr)
    wait_spread_sends(hv, hz, ha, hzs, hzr, hps, hpr)
    wait_mate_sends(xa, xms, xmr)
    wait_mate_sends(ha, hms, hmr)

    def drain(i, carry):
        j = (f + i) % NF
        remote(idt.at[f], idt.at[f], ids_s.at[i], ids_r.at[f], fs=j).wait_send()
        remote(psend.at[j], precv.at[f], p_s.at[j], p_r.at[f], fs=j).wait_send()
        remote(osend.at[j], orecv.at[f], o_s.at[j], o_r.at[f], fs=j).wait_send()
        for n, (src, dst) in enumerate(pieces(j, f)):
            remote(src, dst, w_s.at[n, i], w_r.at[n, f], fs=j).wait_send()
        for n, (src, dst) in enumerate(pieces(f, j)):
            remote(src, dst, w_s.at[n, i], w_r.at[n, j], fs=j).wait_recv()
        return carry

    lax.fori_loop(1, NF, drain, 0)


def solution(mesh):
    NF, NT = mesh.shape["fs"], mesh.shape["tp"]

    def body(tokens, ids, affinity, gain, gt, ut, dt, sgt, sut, sdt):
        TOK, DS = tokens.shape
        E, HS, _ = gt.shape
        EP = E // NF
        EH = E * HS
        NZ = NT // 2
        D = DS * NF
        H = HS * NT
        C = 5 * LANES
        hbm = pl.BlockSpec(memory_space=pl.ANY)
        vmem = pl.BlockSpec(memory_space=pltpu.VMEM)
        dma = pltpu.SemaphoreType.DMA
        outs = pl.pallas_call(
            functools.partial(kernel, NF, NT, D),
            out_shape=(
                jax.ShapeDtypeStruct((TOK, DS), BF16),
                jax.ShapeDtypeStruct((EP * HS, D), BF16),
                jax.ShapeDtypeStruct((EP * HS, D), BF16),
                jax.ShapeDtypeStruct((EP, H, DS), BF16),
                jax.ShapeDtypeStruct((HS, D), BF16),
                jax.ShapeDtypeStruct((HS, D), BF16),
                jax.ShapeDtypeStruct((H, DS), BF16),
            ),
            in_specs=[vmem] * 4 + [hbm] * 3 + [vmem] * 3,
            out_specs=[vmem] + [hbm] * 6,
            scratch_shapes=[
                pltpu.VMEM((3, EH, DS), F32),
                pltpu.VMEM((EH, DS), BF16),
                pltpu.VMEM((EH, DS), BF16),
                pltpu.VMEM((E + EP, HS, DS), BF16),
                pltpu.VMEM((LANES, DS), BF16),
                pltpu.VMEM((4 * LANES, LANES), BF16),
                pltpu.VMEM((16, K * LANES), BF16),
                pltpu.VMEM((TOK, K * HS), F32),
                pltpu.VMEM((NF, 16, TOK), BF16),
                pltpu.VMEM((NZ, TOK, DS), BF16),
                pltpu.VMEM((NF, TOK, DS), BF16),
                pltpu.VMEM((TOK, 3 * LANES), BF16),
                pltpu.VMEM((NZ, TOK, 3 * LANES), BF16),
                pltpu.VMEM((NF, TOK, 3 * LANES), BF16),
                pltpu.VMEM((NF, TOK, K * LANES), BF16),
                pltpu.VMEM((TOK, EH), BF16),
                pltpu.VMEM((TOK, EH), BF16),
                pltpu.VMEM((2, TOK, K * LANES), BF16),
                pltpu.VMEM((TOK, EH + LANES), BF16),
                pltpu.VMEM((NF, TOK, C), BF16),
                pltpu.VMEM((NF, TOK, C), BF16),
                pltpu.VMEM((NF, TOK, DS), BF16),
                pltpu.VMEM((NF, TOK, DS), BF16),
                dma((3,)),
                dma((6,)),
                dma((NF,)),
                dma((NF,)),
                *[dma((NZ,)), dma((NZ,)), dma((NZ,)), dma((NF,)), dma((NF,)), dma((NF,))] * 2,
                *[dma((NF,))] * 4,
                dma((6, NF)),
                dma((6, NF)),
            ],
            compiler_params=pltpu.CompilerParams(
                collective_id=0,
                has_side_effects=True,
                vmem_limit_bytes=60 * 1024 * 1024,
            ),
        )(
            tokens, ids, affinity, gain.reshape(1, DS),
            gt.reshape(EH, DS), ut.reshape(EH, DS), dt.reshape(EH, DS), sgt, sut, sdt,
        )
        mixed, gs, us, ds, sgs, sus, sds = outs
        return mixed, gs.reshape(EP, HS, D), us.reshape(EP, HS, D), ds, sgs, sus, sds

    return jax.shard_map(
        body,
        mesh=mesh,
        in_specs=(
            P("fs", "tp"),
            P("fs", None),
            P("fs", None),
            P("fs"),
            P(None, "tp", "fs"),
            P(None, "tp", "fs"),
            P(None, "fs", "tp"),
            P("tp", "fs"),
            P("tp", "fs"),
            P("fs", "tp"),
        ),
        out_specs=(
            P("fs", "tp"),
            P("fs", "tp", None),
            P("fs", "tp", None),
            P("fs", None, "tp"),
            P("tp", None),
            P("tp", None),
            P(None, "tp"),
        ),
        check_vma=False,
    )
```

time: 283 us -> 185 us (0.65)
  the two profiles are of different devices: /device:TPU:42 before, /device:TPU:13 now
where the time goes in v1:
time: 185 us
  Pallas kernels  174 us (94%)
  local copies, waits for them, and re-layouts  10.8 us (6%)
    pallas_call x1, Pallas kernels, body(): pl.pallas_call(functools.partial(kernel, NF, NT, D), out_shape=(jax.Shape...  174 us
    unnamed x19, local copies, waits for them, and re-layouts  10.8 us

profile of v1, /device:TPU:13, one launch (start us, length us, event | category | flops | bytes accessed | tf_op | source)
XLA Modules:
  0.0 185.1 jit_solution(8690244906865364671)
XLA Ops:
  0.6 1.4 copy.17.ids_ref
  2.0 1.4 copy.18.aff_ref
  3.5 173.6 %shard_map.153 = (bf16[128,256]{1,0:T(8,128)(2,1)}, bf16[128,4096]{1,0:T(8,128)(2,1)}, bf16[128,4096]{1,0:T(8,128)(2,1)}, bf16[4,512,256]{2,1,0:T(8,128)(2,1)}, ...) custom-call(bf16[128,256]{1,0:T(8,128)(2,1)} %tok_ref.1, s32[128,8]{1,0:T(8,128)} %copy.17.ids_ref, ...), custom_call_target="tpu_custom_call" | custom-call | tf_op jit(solution)/shard_map/pallas_call | solution.py:501
  177.1 0.0 copy-start.1
  177.1 1.6 copy.26
  178.6 0.0 copy-start
  178.6 2.4 %copy.27 = bf16[4,32,4096]{2,1,0:T(8,128)(2,1)} copy(bf16[4,32,4096]{2,1,0:T(8,128)(2,1)} %bitcast.10) | data formatting | bytes 2097152
  181.0 0.0 copy-done.1
  181.0 0.0 copy-start.4
  181.0 0.0 copy-start.3
  181.0 0.0 copy-start.2
  181.0 1.0 copy.28
  182.0 0.0 copy-done
  182.0 1.0 copy.29
  183.0 0.0 copy-done.4
  183.0 0.7 copy.30
  183.7 0.0 copy-done.3
  183.7 0.7 copy.31
  184.4 0.0 copy-done.2
  184.4 0.7 copy.32
Async XLA Ops:
  177.1 4.0 %copy-start.1 = (bf16[128,4096]{1,0:T(8,128)(2,1)S(1)}, bf16[128,4096]{1,0:T(8,128)(2,1)}, u32[]{:S(2)}) copy-start(bf16[128,4096]{1,0:T(8,128)(2,1)} %get-tuple-element.16) | copy-start | bytes 3145732
  178.6 3.4 %copy-start = (bf16[4,512,256]{2,1,0:T(8,128)(2,1)S(1)}, bf16[4,512,256]{2,1,0:T(8,128)(2,1)}, u32[]{:S(2)}) copy-start(bf16[4,512,256]{2,1,0:T(8,128)(2,1)} %get-tuple-element.31) | copy-start | bytes 3145732
  181.0 2.0 %copy-start.4 = (bf16[32,4096]{1,0:T(8,128)(2,1)S(1)}, bf16[32,4096]{1,0:T(8,128)(2,1)}, u32[]{:S(2)}) copy-start(bf16[32,4096]{1,0:T(8,128)(2,1)} %get-tuple-element.32) | copy-start | bytes 786436
  181.0 2.7 %copy-start.3 = (bf16[32,4096]{1,0:T(8,128)(2,1)S(1)}, bf16[32,4096]{1,0:T(8,128)(2,1)}, u32[]{:S(2)}) copy-start(bf16[32,4096]{1,0:T(8,128)(2,1)} %get-tuple-element.33) | copy-start | bytes 786436
  181.0 3.4 %copy-start.2 = (bf16[512,256]{1,0:T(8,128)(2,1)S(1)}, bf16[512,256]{1,0:T(8,128)(2,1)}, u32[]{:S(2)}) copy-start(bf16[512,256]{1,0:T(8,128)(2,1)} %get-tuple-element.34) | copy-start | bytes 786436

commit v2 on v1

v2 whole, which is shorter than its diff:
```python
import functools
import math

import jax
import jax.numpy as jnp
from jax import lax
from jax.experimental import pallas as pl
from jax.experimental.pallas import tpu as pltpu
from jax.sharding import PartitionSpec as P

K = 8
NORM_EPS = 1e-06
ROUTED_SCALE = 2.5
LANES = 128
WIDE = 256
F32 = jnp.float32
BF16 = jnp.bfloat16
NT_DIMS = (((1,), (1,)), ((), ()))
TN_DIMS = (((0,), (0,)), ((), ()))


def silu(v):
    return v / (1.0 + jnp.exp(-v))


def kernel(
    NF,
    NT,
    D,
    tok_ref,
    ids_ref,
    aff_ref,
    gain_ref,
    gt_ref,
    ut_ref,
    dt_ref,
    sgt_ref,
    sut_ref,
    sdt_ref,
    mixed_ref,
    gs_ref,
    us_ref,
    ds_ref,
    sgs_ref,
    sus_ref,
    sds_ref,
    wf,
    wg,
    wu,
    wd,
    ws,
    fold,
    spread_ids,
    wexp,
    idt,
    xz,
    xa,
    sq,
    hv,
    hz,
    ha,
    dk,
    gsc,
    usc,
    tsc,
    asc,
    tail_asc,
    psend,
    qa,
    qb,
    sa,
    sb,
    pa,
    pb,
    ptot,
    osend,
    orecv,
    load_sem,
    own_sem,
    ids_s,
    ids_r,
    xzs,
    xzr,
    xps,
    xpr,
    xms,
    xmr,
    hzs,
    hzr,
    hps,
    hpr,
    hms,
    hmr,
    p_s,
    p_r,
    p2_s,
    p2_r,
    o_s,
    o_r,
    w_s,
    w_r,
    sq_s,
    sq_r,
):
    f = lax.axis_index("fs")
    t = lax.axis_index("tp")
    z, c = t // 2, t % 2
    NZ = NT // 2
    TOK, DS = tok_ref.shape
    HS = sgt_ref.shape[0]
    EH = wg.shape[0]
    EP = EH // HS // NF
    GROUPS = EH // WIDE
    ROWS = EP * HS

    loads = []
    for i, r in enumerate((gt_ref, ut_ref, dt_ref)):
        load = pltpu.make_async_copy(r, wf.at[i], load_sem.at[i])
        load.start()
        loads.append(load)

    bar = pltpu.get_barrier_semaphore()

    def greet_plane(i, carry):
        at = (f * 2 + c + i) % (2 * NF)
        pl.semaphore_signal(
            bar, 1, device_id={"fs": at // 2, "tp": z * 2 + at % 2},
            device_id_type=pl.DeviceIdType.MESH,
        )
        return carry

    def greet_column(i, carry):
        pl.semaphore_signal(
            bar, 1, device_id={"tp": ((z + i) % NZ) * 2 + c},
            device_id_type=pl.DeviceIdType.MESH,
        )
        return carry

    lax.fori_loop(1, 2 * NF, greet_plane, 0)
    lax.fori_loop(1, NZ, greet_column, 0)

    idt[f] = jnp.concatenate([ids_ref[...].astype(F32), jnp.zeros((16 - K, TOK), F32)], axis=0).astype(BF16)

    pl.semaphore_wait(bar, 2 * NF - 1 + NZ - 1)

    def remote(src, dst, s, r, **where):
        return pltpu.make_async_remote_copy(
            src_ref=src, dst_ref=dst, send_sem=s, recv_sem=r,
            device_id=where, device_id_type=pl.DeviceIdType.MESH,
        )

    steps = [i for d in range(1, NZ // 2 + 1) for i in dict.fromkeys((d, NZ - d))]

    def along_z(src, stage, s, r):
        for i in steps:
            remote(src, stage.at[z], s.at[i], r.at[z], tp=((z + i) % NZ) * 2 + c).start()

    def in_plane(src, stage, got, zs, zr, s, r, beside=None):
        for n, i in enumerate([0] + [(NZ - i) for i in steps]):
            zz = (z + i) % NZ
            if i:
                remote(src, stage.at[zz], zs.at[i], zr.at[zz], tp=zz * 2 + c).wait_recv()
            part = stage.at[zz] if i else src
            to = zz * 2 + c

            @pl.when(to == f)
            def _():
                got[f] = part[...]

            @pl.when(to != f)
            def _():
                remote(part, got.at[f], s.at[i], r.at[f], fs=to, tp=z * 2 + f % 2).start()

            if beside is not None:
                beside(n)

    def wait_spread_sends(src, stage, got, zs, zr, s, r):
        for i in range(NZ):
            zz = (z + i) % NZ
            to = zz * 2 + c
            if i:
                remote(src, stage.at[z], zs.at[i], zr.at[z], tp=zz * 2 + c).wait_send()

            @pl.when(to != f)
            def _():
                remote(src, got.at[f], s.at[i], r.at[f], fs=to, tp=z * 2 + f % 2).wait_send()

    def direct_block(i):
        return 2 * ((f // 2 + i) % (NF // 2)) + c

    def take_direct(b, got, s, r, ms, mr):
        @pl.when(b != f)
        def _():
            remote(got.at[b], got.at[b], s.at[0], r.at[b], fs=b).wait_recv()

        remote(got.at[b], got.at[b], ms.at[b], mr.at[b], tp=z * 2 + 1 - c).start()

    def take_mate(b, got, ms, mr):
        remote(got.at[b], got.at[b], ms.at[b], mr.at[b], tp=z * 2 + 1 - c).wait_recv()

    def wait_mate_sends(got, ms, mr):
        def body(i, carry):
            b = direct_block(i)
            remote(got.at[b], got.at[b], ms.at[b], mr.at[b], tp=z * 2 + 1 - c).wait_send()
            return carry

        lax.fori_loop(0, NF // 2, body, 0)

    along_z(tok_ref, xz, xzs, xzr)

    def send_ids(i, carry):
        remote(idt.at[f], idt.at[f], ids_s.at[i], ids_r.at[f], fs=(f + i) % NF).start()
        return carry

    lax.fori_loop(1, NF, send_ids, 0)

    fr = lax.broadcasted_iota(jnp.int32, (4 * WIDE, LANES), 0)
    fc = lax.broadcasted_iota(jnp.int32, (4 * WIDE, LANES), 1)
    fold[...] = ((fr // WIDE == fc // HS) & (fr % HS == fc % HS)).astype(BF16)
    sr = lax.broadcasted_iota(jnp.int32, (16, K * WIDE), 0)
    sc = lax.broadcasted_iota(jnp.int32, (16, K * WIDE), 1)
    spread_ids[...] = (sr == sc // WIDE).astype(BF16)

    affinity = aff_ref[...]
    weight = ROUTED_SCALE * affinity / jnp.sum(affinity, axis=0, keepdims=True)
    wr = lax.broadcasted_iota(jnp.int32, (K, K * HS), 0)
    wc = lax.broadcasted_iota(jnp.int32, (K, K * HS), 1)
    place = (wr == wc // HS).astype(BF16)
    high = weight.astype(BF16)
    rest = weight - high.astype(F32)
    middle = rest.astype(BF16)
    low = (rest - middle.astype(F32)).astype(BF16)
    wexp[...] = (
        lax.dot_general(high, place, TN_DIMS, preferred_element_type=F32)
        + lax.dot_general(middle, place, TN_DIMS, preferred_element_type=F32)
        + lax.dot_general(low, place, TN_DIMS, preferred_element_type=F32)
    )

    gain = gain_ref[...]
    ws[...] = jnp.zeros_like(ws)
    ws[0:HS, :DS] = (sgt_ref[...] * gain).astype(BF16)
    ws[HS : 2 * HS, :DS] = (sut_ref[...] * gain).astype(BF16)
    ws[2 * HS :, DS:] = ws[0 : 2 * HS, :DS]
    loads[0].wait()
    loads[1].wait()

    def convert_gate_up(i, carry):
        rows = pl.ds(pl.multiple_of(i * ROWS, ROWS), ROWS)
        wg[rows, :] = (wf[0, rows, :] * gain).astype(BF16)
        wu[rows, :] = (wf[1, rows, :] * gain).astype(BF16)
        return carry

    lax.fori_loop(0, NF, convert_gate_up, 0)

    shared_down = sdt_ref[...].astype(BF16)
    for i in range(LANES // HS):
        wd[EP * NF + i] = shared_down
    loads[2].wait()

    def convert_down(i, carry):
        rows = pl.ds(pl.multiple_of(i * ROWS, ROWS), ROWS)
        wd[pl.ds(i * EP, EP)] = wf[2, rows, :].reshape(EP, HS, DS).astype(BF16)
        return carry

    lax.fori_loop(0, NF, convert_down, 0)

    def pieces(j, src_of):
        cols = pl.ds(pl.multiple_of(src_of * DS, DS), DS)
        rows = pl.ds(pl.multiple_of(j * ROWS, ROWS), ROWS)
        hid = pl.ds(pl.multiple_of(src_of * HS, HS), HS)
        return (
            (wg.at[rows, :], gs_ref.at[:, cols]),
            (wu.at[rows, :], us_ref.at[:, cols]),
            (wd.at[pl.ds(j * EP, EP)], ds_ref.at[:, hid, :]),
            (ws.at[0:HS, 0:DS], sgs_ref.at[:, cols]),
            (ws.at[HS : 2 * HS, 0:DS], sus_ref.at[:, cols]),
            (wd.at[EP * NF], sds_ref.at[hid, :]),
        )

    def send_weights(which, first, last):
        def body(i, carry):
            j = (f + i) % NF
            for n, (src, dst) in enumerate(pieces(j, f)):
                if n in which:
                    remote(src, dst, w_s.at[n, i], w_r.at[n, f], fs=j).start()
            return carry

        lax.fori_loop(first, last, body, 0)

    def pair_of(p):
        def block(i):
            late = i // (NF // 2)
            return 2 * ((f // 2 + i) % (NF // 2)) + (c + late) % 2

        return block(2 * p), block(2 * p + 1)

    def take_ids(b):
        @pl.when(b != f)
        def _():
            remote(idt.at[b], idt.at[b], ids_s.at[0], ids_r.at[b], fs=b).wait_recv()

    def compare(p):
        lane = lax.broadcasted_iota(jnp.int32, (TOK, WIDE), 1)
        quarter = (lane // HS).astype(F32)
        for u, b in enumerate(pair_of(p)):
            take_ids(b)
            ids = lax.dot_general(idt[b], spread_ids[...], TN_DIMS, preferred_element_type=F32)
            for k in range(K):
                dk[p, k, u * TOK : (u + 1) * TOK] = (
                    ids[:, k * WIDE : (k + 1) * WIDE] - quarter
                ).astype(BF16)

    def compare_pairs(n):
        def body(p, carry):
            compare(p)
            return carry

        lax.fori_loop(n * NF // (2 * NZ), (n + 1) * NF // (2 * NZ), body, 0)

    send_weights((0,), 1, NF)
    in_plane(tok_ref, xz, xa, xzs, xzr, xps, xpr, compare_pairs)
    send_weights((3, 4, 5), 1, NF)

    square = jnp.square(tok_ref[...].astype(F32))
    for i in range(1, NZ):
        square = square + jnp.square(xz[(z + i) % NZ].astype(F32))
    sq[0] = jnp.broadcast_to(jnp.sum(square, axis=1, keepdims=True), (TOK, LANES))
    swap = remote(sq.at[0], sq.at[1], sq_s, sq_r, tp=z * 2 + 1 - c)
    swap.start()


    for n, (src, dst) in enumerate(pieces(f, f)):
        pltpu.make_async_copy(src, dst, own_sem.at[n]).start()

    def partial(p):
        b0, b1 = pair_of(p)
        x0, x1 = xa[b0], xa[b1]
        x = jnp.concatenate([x0, x1], axis=0)
        step = 4 * LANES
        for n in range(EH // step):
            part = slice(n * step, (n + 1) * step)
            for w, to in ((wg, gsc), (wu, usc)):
                y = lax.dot_general(x, w[part, :], NT_DIMS, preferred_element_type=F32).astype(BF16)
                for q in range(2):
                    to[2 * n + q] = y[:, q * WIDE : (q + 1) * WIDE]

        def select(r, carry):
            rows = pl.ds(pl.multiple_of(r * 16, 16), 16)
            for k in range(K):
                at = dk[p, k, rows]
                gate = jnp.zeros((16, WIDE), BF16)
                up = jnp.zeros((16, WIDE), BF16)
                for g in range(GROUPS):
                    hit = at == jnp.asarray(WIDE // HS * g, BF16)
                    gate = jnp.where(hit, gsc[g, rows], gate)
                    up = jnp.where(hit, usc[g, rows], up)
                tsc[0, k, rows] = gate
                tsc[1, k, rows] = up
            return carry

        lax.fori_loop(0, 2 * TOK // 16, select, 0)
        for n in range(2):
            for j in range(2):
                at = (2 * n + j) * LANES
                y = jnp.dot(
                    jnp.concatenate([tsc[n, 4 * j + q] for q in range(4)], axis=1),
                    fold[...],
                    preferred_element_type=F32,
                ).astype(BF16)
                psend[b0, :TOK, at : at + LANES] = y[:TOK]
                psend[b1, :TOK, at : at + LANES] = y[TOK:]
        half = TOK // 2
        halves = jnp.concatenate(
            [
                jnp.concatenate([x0[:half], x1[:half]], axis=0),
                jnp.concatenate([x0[half:], x1[half:]], axis=0),
            ],
            axis=1,
        )
        y = lax.dot_general(halves, ws[...], NT_DIMS, preferred_element_type=F32).astype(BF16)
        for q in range(4):
            at = slice(q * LANES, (q + 1) * LANES)
            psend[b0, TOK:, at] = y[16 * q : 16 * q + 16]
            psend[b1, TOK:, at] = y[half + 16 * q : half + 16 * q + 16]

    NX = math.isqrt(NF)
    y, x = f // NX, f % NX
    HALF = (TOK + 16) // 2
    upper, lower = pl.ds(0, HALF), pl.ds(HALF, HALF)

    def upper_copy(b):
        to = y * NX + b % NX
        return remote(
            psend.at[b, upper], qa.at[x, b // NX], p_s.at[0, b], p_r.at[0, x * NX + b // NX], fs=to
        )

    def lower_copy(b):
        to = b // NX * NX + x
        return remote(
            psend.at[b, lower], qb.at[y, b % NX], p_s.at[1, b], p_r.at[1, y * NX + b % NX], fs=to
        )

    def send_partial(b):
        @pl.when(b % NX != x)
        def _():
            upper_copy(b).start()

        @pl.when(b // NX != y)
        def _():
            lower_copy(b).start()

    def add_up(dst, terms):
        for r in range(3):
            at = slice(HALF // 3 * r, HALF // 3 * (r + 1))
            total = terms[0][at].astype(F32)
            for term in terms[1:]:
                total = total + term[at].astype(F32)
            dst[at] = total.astype(dst.dtype)

    def partial_step(p, carry):
        b0, b1 = pair_of(p)
        @pl.when(p < NF // 4)
        def _():
            take_direct(b0, xa, xps, xpr, xms, xmr)
            take_direct(b1, xa, xps, xpr, xms, xmr)

        @pl.when(p >= NF // 4)
        def _():
            take_mate(b0, xa, xms, xmr)
            take_mate(b1, xa, xms, xmr)

        partial(p)
        send_partial(b0)
        send_partial(b1)
        return carry

    lax.fori_loop(0, NF // 2, partial_step, 0)
    swap.wait_recv()

    def second_upper(yb):
        return remote(sa.at[yb], pa.at[y], p2_s.at[0, yb], p2_r.at[0, y], fs=yb * NX + x)

    def second_lower(xb):
        return remote(sb.at[xb], pb.at[x], p2_s.at[1, xb], p2_r.at[1, x], fs=y * NX + xb)

    for i in list(range(1, NX)) + [0]:
        yb, xb = (y + i) % NX, (x + i) % NX
        for j in range(1, NX):
            xs, ys = (x + j) % NX, (y + j) % NX
            remote(
                psend.at[0, upper], qa.at[xs, yb], p_s.at[0, 0], p_r.at[0, xs * NX + yb], fs=f
            ).wait_recv()
            remote(
                psend.at[0, lower], qb.at[ys, xb], p_s.at[1, 0], p_r.at[1, ys * NX + xb], fs=f
            ).wait_recv()
        add_up(
            sa.at[yb],
            [psend.at[yb * NX + x, upper]] + [qa.at[(x + j) % NX, yb] for j in range(1, NX)],
        )
        add_up(
            sb.at[xb],
            [psend.at[y * NX + xb, lower]] + [qb.at[(y + j) % NX, xb] for j in range(1, NX)],
        )
        if i:
            second_upper(yb).start()
            second_lower(xb).start()
    pass
    for i in range(1, NX):
        ys, xs = (y + i) % NX, (x + i) % NX
        remote(sa.at[0], pa.at[ys], p2_s.at[0, 0], p2_r.at[0, ys], fs=f).wait_recv()
        remote(sb.at[0], pb.at[xs], p2_s.at[1, 0], p2_r.at[1, xs], fs=f).wait_recv()
    add_up(ptot.at[upper], [sa.at[y]] + [pa.at[(y + i) % NX] for i in range(1, NX)])
    add_up(ptot.at[lower], [sb.at[x]] + [pb.at[(x + i) % NX] for i in range(1, NX)])

    def summed(mine, got, rows):
        total = mine[f, rows, :].astype(F32)
        for i in range(1, NF):
            total = total + got[(f + i) % NF, rows, :].astype(F32)
        return total

    half = K * HS
    inverse_rms = lax.rsqrt((sq[0] + sq[1]) * (1.0 / D) + NORM_EPS)
    for r in range(TOK // 16):
        rows = slice(16 * r, 16 * r + 16)
        total = ptot[rows, :]
        inv = jnp.concatenate([inverse_rms[rows]] * (half // LANES), axis=1)
        hidden = silu(total[:, :half] * inv) * (total[:, half:] * inv) * wexp[rows, :]
        hv[rows, :] = hidden.astype(BF16)
    lane = lax.broadcasted_iota(jnp.int32, (16, LANES), 1)
    total = ptot[TOK:, :]
    low, high = jnp.zeros((16, LANES), F32), jnp.zeros((16, LANES), F32)
    for q in range(4):
        inv = jnp.where(
            lane < 2 * HS,
            inverse_rms[16 * q : 16 * q + 16],
            inverse_rms[16 * q + TOK // 2 : 16 * q + TOK // 2 + 16],
        )
        pre = total[:, q * LANES : (q + 1) * LANES] * inv
        shared = silu(pre) * pltpu.roll(pre, LANES - HS, 1)
        here = lane // HS == q
        first = pltpu.roll(shared, HS * q, 1) if q else shared
        second = pltpu.roll(shared, (HS * q + 2 * HS) % LANES, 1) if q != 2 else shared
        low = jnp.where(here, first, low)
        high = jnp.where(here, second, high)
    hv[TOK:, :LANES] = low.astype(BF16)
    hv[TOK:, LANES:] = high.astype(BF16)

    along_z(hv, hz, hzs, hzr)
    send_weights((1,), 1, NF)
    in_plane(hv, hz, ha, hzs, hzr, hps, hpr)
    send_weights((2,), 1, NF)

    pass

    def down(p):
        b0, b1 = pair_of(p)
        for j in range(2):
            at = slice(j * LANES, (j + 1) * LANES)
            y = lax.dot_general(
                jnp.concatenate([ha[b0, :TOK, at], ha[b1, :TOK, at]], axis=0),
                fold[...],
                NT_DIMS,
                preferred_element_type=F32,
            ).astype(BF16)
            for q in range(4):
                tsc[0, 4 * j + q] = y[:, q * WIDE : (q + 1) * WIDE]

        def scatter(r, carry):
            rows = pl.ds(pl.multiple_of(r * 16, 16), 16)
            at = [dk[p, k, rows] for k in range(K)]
            hid = [tsc[0, k, rows] for k in range(K)]
            for g in range(GROUPS):
                a = jnp.zeros((16, WIDE), BF16)
                for k in range(K):
                    a = jnp.where(at[k] == jnp.asarray(WIDE // HS * g, BF16), hid[k], a)
                asc[g, rows] = a
            b = b0 + (r // (TOK // 16)) * (b1 - b0)
            s = r % (TOK // 16)
            tail = ha[b, TOK:, pl.ds(pl.multiple_of(s // 4 * LANES, LANES), LANES)]
            lane = lax.broadcasted_iota(jnp.int32, (16, LANES), 1)
            tail_asc[rows] = jnp.where(lane // HS == s % 4, tail.astype(F32), 0.0).astype(BF16)
            return carry

        lax.fori_loop(0, 2 * TOK // 16, scatter, 0)
        y = jnp.dot(
            jnp.concatenate([asc[g] for g in range(GROUPS)] + [tail_asc[...]], axis=1),
            wd[...].reshape(EH + LANES, DS),
            preferred_element_type=F32,
        ).astype(BF16)
        osend[b0] = y[:TOK]
        osend[b1] = y[TOK:]

    def send_out(b):
        @pl.when(b != f)
        def _():
            remote(osend.at[b], orecv.at[f], o_s.at[b], o_r.at[f], fs=b).start()

    def down_step(p, carry):
        b0, b1 = pair_of(p)

        @pl.when(p < NF // 4)
        def _():
            take_direct(b0, ha, hps, hpr, hms, hmr)
            take_direct(b1, ha, hps, hpr, hms, hmr)

        @pl.when(p >= NF // 4)
        def _():
            take_mate(b0, ha, hms, hmr)
            take_mate(b1, ha, hms, hmr)

        down(p)
        send_out(b0)
        send_out(b1)
        return carry

    lax.fori_loop(0, NF // 2, down_step, 0)

    def take_out(i, carry):
        j = (f + i) % NF
        remote(osend.at[j], orecv.at[j], o_s.at[j], o_r.at[j], fs=j).wait_recv()
        return carry

    lax.fori_loop(1, NF, take_out, 0)

    def finish(r, carry):
        rows = pl.ds(pl.multiple_of(r * 16, 16), 16)
        mixed_ref[rows, :] = summed(osend, orecv, rows).astype(BF16)
        return carry

    lax.fori_loop(0, TOK // 16, finish, 0)

    swap.wait_send()
    for n, (src, dst) in enumerate(pieces(f, f)):
        pltpu.make_async_copy(src, dst, own_sem.at[n]).wait()
    wait_spread_sends(tok_ref, xz, xa, xzs, xzr, xps, xpr)
    wait_spread_sends(hv, hz, ha, hzs, hzr, hps, hpr)
    wait_mate_sends(xa, xms, xmr)
    wait_mate_sends(ha, hms, hmr)

    def drain(i, carry):
        j = (f + i) % NF
        remote(idt.at[f], idt.at[f], ids_s.at[i], ids_r.at[f], fs=j).wait_send()
        remote(osend.at[j], orecv.at[f], o_s.at[j], o_r.at[f], fs=j).wait_send()
        for n, (src, dst) in enumerate(pieces(j, f)):
            remote(src, dst, w_s.at[n, i], w_r.at[n, f], fs=j).wait_send()
        for n, (src, dst) in enumerate(pieces(f, j)):
            remote(src, dst, w_s.at[n, i], w_r.at[n, j], fs=j).wait_recv()
        return carry

    lax.fori_loop(1, NF, drain, 0)

    def drain_partial(b, carry):
        @pl.when(b % NX != x)
        def _():
            upper_copy(b).wait_send()

        @pl.when(b // NX != y)
        def _():
            lower_copy(b).wait_send()

        return carry

    lax.fori_loop(0, NF, drain_partial, 0)
    for i in range(1, NX):
        second_upper((y + i) % NX).wait_send()
        second_lower((x + i) % NX).wait_send()


def place(n, *refs):
    src, dst, held, s_in, s_out = refs[:n], refs[n : 2 * n], refs[2 * n : 3 * n], refs[-2], refs[-1]
    parts = []
    for a, b, h in zip(src, dst, held):
        rows = a.shape[0]
        cuts = 4 if rows % 64 == 0 and a.shape[-1] * rows > 1 << 18 else 1
        for i in range(cuts):
            at = pl.ds(rows // cuts * i, rows // cuts)
            parts.append((a.at[at], b.at[at], h.at[at]))
    for i, (a, b, h) in enumerate(parts):
        pltpu.make_async_copy(a, h, s_in.at[i]).start()
    for i, (a, b, h) in enumerate(parts):
        pltpu.make_async_copy(a, h, s_in.at[i]).wait()
        pltpu.make_async_copy(h, b, s_out.at[i]).start()
    for i, (a, b, h) in enumerate(parts):
        pltpu.make_async_copy(h, b, s_out.at[i]).wait()


def solution(mesh):
    NF, NT = mesh.shape["fs"], mesh.shape["tp"]

    def body(tokens, ids, affinity, gain, gt, ut, dt, sgt, sut, sdt):
        TOK, DS = tokens.shape
        E, HS, _ = gt.shape
        EP = E // NF
        EH = E * HS
        NZ = NT // 2
        NX = math.isqrt(NF)
        D = DS * NF
        H = HS * NT
        hbm = pl.BlockSpec(memory_space=pl.ANY)
        vmem = pl.BlockSpec(memory_space=pltpu.VMEM)
        dma = pltpu.SemaphoreType.DMA
        outs = pl.pallas_call(
            functools.partial(kernel, NF, NT, D),
            out_shape=(
                jax.ShapeDtypeStruct((TOK, DS), BF16),
                jax.ShapeDtypeStruct((EP * HS, D), BF16),
                jax.ShapeDtypeStruct((EP * HS, D), BF16),
                jax.ShapeDtypeStruct((EP, H, DS), BF16),
                jax.ShapeDtypeStruct((HS, D), BF16),
                jax.ShapeDtypeStruct((HS, D), BF16),
                jax.ShapeDtypeStruct((H, DS), BF16),
            ),
            in_specs=[vmem] * 4 + [hbm] * 3 + [vmem] * 3,
            out_specs=[vmem] + [hbm] * 6,
            scratch_shapes=[
                pltpu.VMEM((3, EH, DS), F32),
                pltpu.VMEM((EH, DS), BF16),
                pltpu.VMEM((EH, DS), BF16),
                pltpu.VMEM((E + LANES // HS, HS, DS), BF16),
                pltpu.VMEM((LANES, 2 * DS), BF16),
                pltpu.VMEM((4 * WIDE, LANES), BF16),
                pltpu.VMEM((16, K * WIDE), BF16),
                pltpu.VMEM((TOK, K * HS), F32),
                pltpu.VMEM((NF, 16, TOK), BF16),
                pltpu.VMEM((NZ, TOK, DS), BF16),
                pltpu.VMEM((NF, TOK, DS), BF16),
                pltpu.VMEM((2, TOK, LANES), F32),
                pltpu.VMEM((TOK + 16, K * HS), BF16),
                pltpu.VMEM((NZ, TOK + 16, K * HS), BF16),
                pltpu.VMEM((NF, TOK + 16, K * HS), BF16),
                pltpu.VMEM((NF // 2, K, 2 * TOK, WIDE), BF16),
                pltpu.VMEM((EH // WIDE, 2 * TOK, WIDE), BF16),
                pltpu.VMEM((EH // WIDE, 2 * TOK, WIDE), BF16),
                pltpu.VMEM((2, K, 2 * TOK, WIDE), BF16),
                pltpu.VMEM((EH // WIDE, 2 * TOK, WIDE), BF16),
                pltpu.VMEM((2 * TOK, LANES), BF16),
                pltpu.VMEM((NF, TOK + 16, 2 * K * HS), BF16),
                *[pltpu.VMEM((NX, NX, (TOK + 16) // 2, 2 * K * HS), BF16)] * 2,
                *[pltpu.VMEM((NX, (TOK + 16) // 2, 2 * K * HS), BF16)] * 4,
                pltpu.VMEM((TOK + 16, 2 * K * HS), F32),
                pltpu.VMEM((NF, TOK, DS), BF16),
                pltpu.VMEM((NF, TOK, DS), BF16),
                dma((3,)),
                dma((6,)),
                dma((NF,)),
                dma((NF,)),
                *[dma((NZ,)), dma((NZ,)), dma((NZ,)), dma((NF,)), dma((NF,)), dma((NF,))] * 2,
                *[dma((2, NF))] * 2,
                *[dma((2, NX))] * 2,
                *[dma((NF,))] * 2,
                dma((6, NF)),
                dma((6, NF)),
                dma,
                dma,
            ],
            compiler_params=pltpu.CompilerParams(
                collective_id=0,
                has_side_effects=True,
                vmem_limit_bytes=60 * 1024 * 1024,
            ),
        )(
            tokens, ids.T, affinity.T, gain.reshape(1, DS),
            gt.reshape(EH, DS), ut.reshape(EH, DS), dt.reshape(EH, DS), sgt, sut, sdt,
        )
        n = len(outs)
        outs = (*outs[:3], outs[3].reshape(EP * H, DS), *outs[4:])
        shapes = [jax.ShapeDtypeStruct(a.shape, a.dtype) for a in outs]
        outs = pl.pallas_call(
            functools.partial(place, n),
            out_shape=shapes,
            in_specs=[hbm] * n,
            out_specs=[hbm] * n,
            scratch_shapes=[pltpu.VMEM(a.shape, a.dtype) for a in shapes] + [dma((4 * n,))] * 2,
            compiler_params=pltpu.CompilerParams(vmem_limit_bytes=60 * 1024 * 1024),
        )(*outs)
        mixed, gs, us, ds, sgs, sus, sds = outs
        ds = ds.reshape(EP, H, DS)
        return mixed, gs.reshape(EP, HS, D), us.reshape(EP, HS, D), ds, sgs, sus, sds

    return jax.shard_map(
        body,
        mesh=mesh,
        in_specs=(
            P("fs", "tp"),
            P("fs", None),
            P("fs", None),
            P("fs"),
            P(None, "tp", "fs"),
            P(None, "tp", "fs"),
            P(None, "fs", "tp"),
            P("tp", "fs"),
            P("tp", "fs"),
            P("fs", "tp"),
        ),
        out_specs=(
            P("fs", "tp"),
            P("fs", "tp", None),
            P("fs", "tp", None),
            P("fs", None, "tp"),
            P("tp", None),
            P("tp", None),
            P(None, "tp"),
        ),
        check_vma=False,
    )
```

time: 185 us -> 133 us (0.72)
  the two profiles are of different devices: /device:TPU:13 before, /device:TPU:42 now
where the time goes in v2:
time: 133 us
  Pallas kernels  132 us (99%)
    pallas_call x1, Pallas kernels, body(): pl.pallas_call(functools.partial(kernel, NF, NT, D), out_shape=(jax.Shape...  128 us
    pallas_call x1, Pallas kernels, body(): pl.pallas_call(functools.partial(place, n), out_shape=shapes, in_specs=[h...  3.88 us

profile of v2, /device:TPU:42, one launch (start us, length us, event | category | flops | bytes accessed | tf_op | source)
XLA Modules:
  0.0 132.9 jit_solution(3937203880031781825)
XLA Ops:
  0.6 128.3 %shard_map.153 = (bf16[128,256]{1,0:T(8,128)(2,1)}, bf16[128,4096]{1,0:T(8,128)(2,1)}, bf16[128,4096]{1,0:T(8,128)(2,1)}, bf16[4,512,256]{2,1,0:T(8,128)(2,1)}, ...) custom-call(bf16[128,256]{1,0:T(8,128)(2,1)} %tok_ref.1, s32[8,128]{1,0:T(8,128)} %bitcast.14, ...), custom_call_target="tpu_custom_call" | custom-call | tf_op jit(solution)/shard_map/pallas_call | solution.py:662
  129.0 3.9 %shard_map.154 = (bf16[128,256]{1,0:T(8,128)(2,1)}, bf16[128,4096]{1,0:T(8,128)(2,1)}, bf16[128,4096]{1,0:T(8,128)(2,1)}, bf16[2048,256]{1,0:T(8,128)(2,1)}, bf1...) custom-call(bf16[128,256]{1,0:T(8,128)(2,1)} %get-tuple-element.21.refs_0_, ...), custom_call_target="tpu_custom_call" | custom-call | tf_op jit(solution)/shard_map/pallas_call | solution.py:728

commit v3 on v2

--- a/solution.py
+++ b/solution.py
@@ -12,7 +12,6 @@
 NORM_EPS = 1e-06
 ROUTED_SCALE = 2.5
 LANES = 128
-WIDE = 256
 F32 = jnp.float32
 BF16 = jnp.bfloat16
 NT_DIMS = (((1,), (1,)), ((), ()))
@@ -49,7 +48,9 @@
     wu,
     wd,
     ws,
-    fold,
+    wgp,
+    wup,
+    wdp,
     spread_ids,
     wexp,
     idt,
@@ -59,10 +60,9 @@
     hv,
     hz,
     ha,
-    dk,
-    gsc,
-    usc,
-    tsc,
+    choice,
+    expert,
+    pre,
     asc,
     tail_asc,
     psend,
@@ -110,14 +110,18 @@
     HS = sgt_ref.shape[0]
     EH = wg.shape[0]
     EP = EH // HS // NF
-    GROUPS = EH // WIDE
+    TILES = EH // LANES
+    E = EP * NF
     ROWS = EP * HS
 
     loads = []
     for i, r in enumerate((gt_ref, ut_ref, dt_ref)):
-        load = pltpu.make_async_copy(r, wf.at[i], load_sem.at[i])
-        load.start()
-        loads.append(load)
+        for q in range(DS // LANES):
+            load = pltpu.make_async_copy(
+                r.at[:, q * LANES : (q + 1) * LANES], wf.at[2 * i + q], load_sem.at[2 * i + q]
+            )
+            load.start()
+            loads.append(load)
 
     bar = pltpu.get_barrier_semaphore()
 
@@ -214,18 +218,16 @@
 
     lax.fori_loop(1, NF, send_ids, 0)
 
-    fr = lax.broadcasted_iota(jnp.int32, (4 * WIDE, LANES), 0)
-    fc = lax.broadcasted_iota(jnp.int32, (4 * WIDE, LANES), 1)
-    fold[...] = ((fr // WIDE == fc // HS) & (fr % HS == fc % HS)).astype(BF16)
-    sr = lax.broadcasted_iota(jnp.int32, (16, K * WIDE), 0)
-    sc = lax.broadcasted_iota(jnp.int32, (16, K * WIDE), 1)
-    spread_ids[...] = (sr == sc // WIDE).astype(BF16)
+    sr = lax.broadcasted_iota(jnp.int32, (16, K * LANES), 0)
+    sc = lax.broadcasted_iota(jnp.int32, (16, K * LANES), 1)
+    spread_ids[:, : K * LANES] = (sr == sc // LANES).astype(BF16)
+    spread_ids[:, K * LANES :] = (sr[:, :LANES] == sc[:, :LANES] % K).astype(BF16)
 
     affinity = aff_ref[...]
     weight = ROUTED_SCALE * affinity / jnp.sum(affinity, axis=0, keepdims=True)
     wr = lax.broadcasted_iota(jnp.int32, (K, K * HS), 0)
     wc = lax.broadcasted_iota(jnp.int32, (K, K * HS), 1)
-    place = (wr == wc // HS).astype(BF16)
+    place = (wr == wc % K).astype(BF16)
     high = weight.astype(BF16)
     rest = weight - high.astype(F32)
     middle = rest.astype(BF16)
@@ -241,28 +243,48 @@
     ws[0:HS, :DS] = (sgt_ref[...] * gain).astype(BF16)
     ws[HS : 2 * HS, :DS] = (sut_ref[...] * gain).astype(BF16)
     ws[2 * HS :, DS:] = ws[0 : 2 * HS, :DS]
-    loads[0].wait()
-    loads[1].wait()
+    for load in loads[:4]:
+        load.wait()
+    halves = [slice(q * LANES, (q + 1) * LANES) for q in range(DS // LANES)]
 
     def convert_gate_up(i, carry):
         rows = pl.ds(pl.multiple_of(i * ROWS, ROWS), ROWS)
-        wg[rows, :] = (wf[0, rows, :] * gain).astype(BF16)
-        wu[rows, :] = (wf[1, rows, :] * gain).astype(BF16)
+        for q, at in enumerate(halves):
+            wg[rows, at] = (wf[q, rows, :] * gain[:, at]).astype(BF16)
+            wu[rows, at] = (wf[2 + q, rows, :] * gain[:, at]).astype(BF16)
         return carry
 
     lax.fori_loop(0, NF, convert_gate_up, 0)
 
+    def reorder_gate_up(h, carry):
+        rows = pl.ds(pl.multiple_of(h * E, E), E)
+        for q, at in enumerate(halves):
+            wgp[rows, at] = (wf[q, pl.ds(h, E, stride=HS), :] * gain[:, at]).astype(BF16)
+            wup[rows, at] = (wf[2 + q, pl.ds(h, E, stride=HS), :] * gain[:, at]).astype(BF16)
+        return carry
+
+
     shared_down = sdt_ref[...].astype(BF16)
-    for i in range(LANES // HS):
-        wd[EP * NF + i] = shared_down
-    loads[2].wait()
+    wd[E] = shared_down
+    for load in loads[4:]:
+        load.wait()
 
     def convert_down(i, carry):
         rows = pl.ds(pl.multiple_of(i * ROWS, ROWS), ROWS)
-        wd[pl.ds(i * EP, EP)] = wf[2, rows, :].reshape(EP, HS, DS).astype(BF16)
+        for q, at in enumerate(halves):
+            wd[pl.ds(i * EP, EP), :, at] = wf[4 + q, rows, :].reshape(EP, HS, LANES).astype(BF16)
         return carry
 
     lax.fori_loop(0, NF, convert_down, 0)
+    for i in range(LANES // HS):
+        wdp[EH + i * HS : EH + (i + 1) * HS, :] = shared_down
+
+    def reorder_down(h, carry):
+        rows = pl.ds(pl.multiple_of(h * E, E), E)
+        for q, at in enumerate(halves):
+            wdp[rows, at] = wf[4 + q, pl.ds(h, E, stride=HS), :].astype(BF16)
+        return carry
+
 
     def pieces(j, src_of):
         cols = pl.ds(pl.multiple_of(src_of * DS, DS), DS)
@@ -279,7 +301,7 @@
 
     def send_weights(which, first, last):
         def body(i, carry):
-            j = (f + i) % NF
+            j = (f + i + c * (NF - 2 * i)) % NF
             for n, (src, dst) in enumerate(pieces(j, f)):
                 if n in which:
                     remote(src, dst, w_s.at[n, i], w_r.at[n, f], fs=j).start()
@@ -300,15 +322,17 @@
             remote(idt.at[b], idt.at[b], ids_s.at[0], ids_r.at[b], fs=b).wait_recv()
 
     def compare(p):
-        lane = lax.broadcasted_iota(jnp.int32, (TOK, WIDE), 1)
-        quarter = (lane // HS).astype(F32)
-        for u, b in enumerate(pair_of(p)):
+        lane = lax.broadcasted_iota(jnp.int32, (TOK, LANES), 1)
+        for b in pair_of(p):
             take_ids(b)
-            ids = lax.dot_general(idt[b], spread_ids[...], TN_DIMS, preferred_element_type=F32)
+            ids = lax.dot_general(
+                idt[b], spread_ids[...], TN_DIMS, preferred_element_type=F32
+            ).astype(jnp.int32)
+            choice[b] = (lane // K) % (LANES // E) * E + ids[:, K * LANES :]
+            at = jnp.full((TOK, LANES), -1, jnp.int32)
             for k in range(K):
-                dk[p, k, u * TOK : (u + 1) * TOK] = (
-                    ids[:, k * WIDE : (k + 1) * WIDE] - quarter
-                ).astype(BF16)
+                at = jnp.where(ids[:, k * LANES : (k + 1) * LANES] == lane % E, lane // E * K + k, at)
+            expert[b] = at
 
     def compare_pairs(n):
         def body(p, carry):
@@ -316,6 +340,8 @@
             return carry
 
         lax.fori_loop(n * NF // (2 * NZ), (n + 1) * NF // (2 * NZ), body, 0)
+        lax.fori_loop(n * HS // NZ, (n + 1) * HS // NZ, reorder_gate_up, 0)
+        lax.fori_loop(n * HS // NZ, (n + 1) * HS // NZ, reorder_down, 0)
 
     send_weights((0,), 1, NF)
     in_plane(tok_ref, xz, xa, xzs, xzr, xps, xpr, compare_pairs)
@@ -339,45 +365,40 @@
         step = 4 * LANES
         for n in range(EH // step):
             part = slice(n * step, (n + 1) * step)
-            for w, to in ((wg, gsc), (wu, usc)):
-                y = lax.dot_general(x, w[part, :], NT_DIMS, preferred_element_type=F32).astype(BF16)
-                for q in range(2):
-                    to[2 * n + q] = y[:, q * WIDE : (q + 1) * WIDE]
-
-        def select(r, carry):
-            rows = pl.ds(pl.multiple_of(r * 16, 16), 16)
-            for k in range(K):
-                at = dk[p, k, rows]
-                gate = jnp.zeros((16, WIDE), BF16)
-                up = jnp.zeros((16, WIDE), BF16)
-                for g in range(GROUPS):
-                    hit = at == jnp.asarray(WIDE // HS * g, BF16)
-                    gate = jnp.where(hit, gsc[g, rows], gate)
-                    up = jnp.where(hit, usc[g, rows], up)
-                tsc[0, k, rows] = gate
-                tsc[1, k, rows] = up
+            for i, w in enumerate((wgp, wup)):
+                y = lax.dot_general(x, w[part, :], NT_DIMS, preferred_element_type=F32)
+                for q in range(4):
+                    pre[i * TILES + 4 * n + q] = y[:, q * LANES : (q + 1) * LANES]
+        per = LANES // (K * (LANES // E))
+
+        lane = lax.broadcasted_iota(jnp.int32, (16, LANES), 1)
+        group = lane // (LANES // per)
+
+        def select(m, carry):
+            for u in range(4):
+                r = 4 * m + u
+                rows = pl.ds(pl.multiple_of(r * 16, 16), 16)
+                b = b0 + r // (TOK // 16) * (b1 - b0)
+                here = pl.ds(pl.multiple_of(r % (TOK // 16) * 16, 16), 16)
+                at = choice[b, here]
+                for o in range(2 * TILES // per):
+                    total = jnp.take_along_axis(pre[o * per, rows], at, axis=1)
+                    for j in range(1, per):
+                        value = jnp.take_along_axis(pre[o * per + j, rows], at, axis=1)
+                        total = jnp.where(group == j, value, total)
+                    psend[b, here, o * LANES : (o + 1) * LANES] = total.astype(BF16)
             return carry
 
-        lax.fori_loop(0, 2 * TOK // 16, select, 0)
-        for n in range(2):
-            for j in range(2):
-                at = (2 * n + j) * LANES
-                y = jnp.dot(
-                    jnp.concatenate([tsc[n, 4 * j + q] for q in range(4)], axis=1),
-                    fold[...],
-                    preferred_element_type=F32,
-                ).astype(BF16)
-                psend[b0, :TOK, at : at + LANES] = y[:TOK]
-                psend[b1, :TOK, at : at + LANES] = y[TOK:]
+        lax.fori_loop(0, 2 * TOK // 64, select, 0)
         half = TOK // 2
-        halves = jnp.concatenate(
+        two = jnp.concatenate(
             [
                 jnp.concatenate([x0[:half], x1[:half]], axis=0),
                 jnp.concatenate([x0[half:], x1[half:]], axis=0),
             ],
             axis=1,
         )
-        y = lax.dot_general(halves, ws[...], NT_DIMS, preferred_element_type=F32).astype(BF16)
+        y = lax.dot_general(two, ws[...], NT_DIMS, preferred_element_type=F32).astype(BF16)
         for q in range(4):
             at = slice(q * LANES, (q + 1) * LANES)
             psend[b0, TOK:, at] = y[16 * q : 16 * q + 16]
@@ -507,44 +528,40 @@
 
     along_z(hv, hz, hzs, hzr)
     send_weights((1,), 1, NF)
+    send_weights((2,), 1, NF)
     in_plane(hv, hz, ha, hzs, hzr, hps, hpr)
-    send_weights((2,), 1, NF)
 
     pass
 
     def down(p):
         b0, b1 = pair_of(p)
-        for j in range(2):
-            at = slice(j * LANES, (j + 1) * LANES)
-            y = lax.dot_general(
-                jnp.concatenate([ha[b0, :TOK, at], ha[b1, :TOK, at]], axis=0),
-                fold[...],
-                NT_DIMS,
-                preferred_element_type=F32,
-            ).astype(BF16)
-            for q in range(4):
-                tsc[0, 4 * j + q] = y[:, q * WIDE : (q + 1) * WIDE]
-
-        def scatter(r, carry):
-            rows = pl.ds(pl.multiple_of(r * 16, 16), 16)
-            at = [dk[p, k, rows] for k in range(K)]
-            hid = [tsc[0, k, rows] for k in range(K)]
-            for g in range(GROUPS):
-                a = jnp.zeros((16, WIDE), BF16)
-                for k in range(K):
-                    a = jnp.where(at[k] == jnp.asarray(WIDE // HS * g, BF16), hid[k], a)
-                asc[g, rows] = a
-            b = b0 + (r // (TOK // 16)) * (b1 - b0)
-            s = r % (TOK // 16)
-            tail = ha[b, TOK:, pl.ds(pl.multiple_of(s // 4 * LANES, LANES), LANES)]
-            lane = lax.broadcasted_iota(jnp.int32, (16, LANES), 1)
-            tail_asc[rows] = jnp.where(lane // HS == s % 4, tail.astype(F32), 0.0).astype(BF16)
+        per = LANES // (K * (LANES // E))
+
+        lane = lax.broadcasted_iota(jnp.int32, (16, LANES), 1)
+
+        def scatter(m, carry):
+            for u in range(4):
+                r = 4 * m + u
+                rows = pl.ds(pl.multiple_of(r * 16, 16), 16)
+                b = b0 + r // (TOK // 16) * (b1 - b0)
+                s = r % (TOK // 16)
+                here = pl.ds(pl.multiple_of(s * 16, 16), 16)
+                at = expert[b, here]
+                chosen = at >= 0
+                at = jnp.maximum(at, 0)
+                for o in range(TILES // per):
+                    hidden = ha[b, here, o * LANES : (o + 1) * LANES].astype(F32)
+                    for j in range(per):
+                        value = jnp.take_along_axis(hidden, at + j * (LANES // per), axis=1)
+                        asc[o * per + j, rows] = jnp.where(chosen, value, 0.0).astype(BF16)
+                tail = ha[b, TOK:, pl.ds(pl.multiple_of(s // 4 * LANES, LANES), LANES)]
+                tail_asc[rows] = jnp.where(lane // HS == s % 4, tail.astype(F32), 0.0).astype(BF16)
             return carry
 
-        lax.fori_loop(0, 2 * TOK // 16, scatter, 0)
+        lax.fori_loop(0, 2 * TOK // 64, scatter, 0)
         y = jnp.dot(
-            jnp.concatenate([asc[g] for g in range(GROUPS)] + [tail_asc[...]], axis=1),
-            wd[...].reshape(EH + LANES, DS),
+            jnp.concatenate([asc[g] for g in range(TILES)] + [tail_asc[...]], axis=1),
+            wdp[...],
             preferred_element_type=F32,
         ).astype(BF16)
         osend[b0] = y[:TOK]
@@ -673,13 +690,15 @@
             in_specs=[vmem] * 4 + [hbm] * 3 + [vmem] * 3,
             out_specs=[vmem] + [hbm] * 6,
             scratch_shapes=[
-                pltpu.VMEM((3, EH, DS), F32),
+                pltpu.VMEM((6, EH, LANES), F32),
                 pltpu.VMEM((EH, DS), BF16),
                 pltpu.VMEM((EH, DS), BF16),
-                pltpu.VMEM((E + LANES // HS, HS, DS), BF16),
+                pltpu.VMEM((E + 1, HS, DS), BF16),
                 pltpu.VMEM((LANES, 2 * DS), BF16),
-                pltpu.VMEM((4 * WIDE, LANES), BF16),
-                pltpu.VMEM((16, K * WIDE), BF16),
+                pltpu.VMEM((EH, DS), BF16),
+                pltpu.VMEM((EH, DS), BF16),
+                pltpu.VMEM((EH + LANES, DS), BF16),
+                pltpu.VMEM((16, (K + 1) * LANES), BF16),
                 pltpu.VMEM((TOK, K * HS), F32),
                 pltpu.VMEM((NF, 16, TOK), BF16),
                 pltpu.VMEM((NZ, TOK, DS), BF16),
@@ -688,11 +707,10 @@
                 pltpu.VMEM((TOK + 16, K * HS), BF16),
                 pltpu.VMEM((NZ, TOK + 16, K * HS), BF16),
                 pltpu.VMEM((NF, TOK + 16, K * HS), BF16),
-                pltpu.VMEM((NF // 2, K, 2 * TOK, WIDE), BF16),
-                pltpu.VMEM((EH // WIDE, 2 * TOK, WIDE), BF16),
-                pltpu.VMEM((EH // WIDE, 2 * TOK, WIDE), BF16),
-                pltpu.VMEM((2, K, 2 * TOK, WIDE), BF16),
-                pltpu.VMEM((EH // WIDE, 2 * TOK, WIDE), BF16),
+                pltpu.VMEM((NF, TOK, LANES), jnp.int32),
+                pltpu.VMEM((NF, TOK, LANES), jnp.int32),
+                pltpu.VMEM((2 * EH // LANES, 2 * TOK, LANES), F32),
+                pltpu.VMEM((EH // LANES, 2 * TOK, LANES), BF16),
                 pltpu.VMEM((2 * TOK, LANES), BF16),
                 pltpu.VMEM((NF, TOK + 16, 2 * K * HS), BF16),
                 *[pltpu.VMEM((NX, NX, (TOK + 16) // 2, 2 * K * HS), BF16)] * 2,
@@ -700,7 +718,7 @@
                 pltpu.VMEM((TOK + 16, 2 * K * HS), F32),
                 pltpu.VMEM((NF, TOK, DS), BF16),
                 pltpu.VMEM((NF, TOK, DS), BF16),
-                dma((3,)),
+                dma((6,)),
                 dma((6,)),
                 dma((NF,)),
                 dma((NF,)),

time: 133 us -> 126 us (0.947); the launches traced: 133 us -> 123 us
  Pallas kernels: 132 us -> 123 us
    pallas_call x1, Pallas kernels: 128 us -> 119 us  [body(): pl.pallas_call(functools.partial(kernel, NF, NT, D), out_shape=(jax.Shape...]
where the time goes in v3:
time: 126 us; the launch traced here: 123 us
  Pallas kernels  123 us (98%)
    pallas_call x1, Pallas kernels, body(): pl.pallas_call(functools.partial(kernel, NF, NT, D), out_shape=(jax.Shape...  119 us
    pallas_call x1, Pallas kernels, body(): pl.pallas_call(functools.partial(place, n), out_shape=shapes, in_specs=[h...  3.88 us

profile of v3, /device:TPU:42, one launch (start us, length us, event | category | flops | bytes accessed | tf_op | source)
XLA Modules:
  0.0 123.2 jit_solution(13237784755336452146)
XLA Ops:
  0.6 118.7 %shard_map.153 = (bf16[128,256]{1,0:T(8,128)(2,1)}, bf16[128,4096]{1,0:T(8,128)(2,1)}, bf16[128,4096]{1,0:T(8,128)(2,1)}, bf16[4,512,256]{2,1,0:T(8,128)(2,1)}, ...) custom-call(bf16[128,256]{1,0:T(8,128)(2,1)} %tok_ref.1, s32[8,128]{1,0:T(8,128)} %bitcast.14, ...), custom_call_target="tpu_custom_call" | custom-call | tf_op jit(solution)/shard_map/pallas_call | solution.py:679
  119.4 3.9 %shard_map.154 = (bf16[128,256]{1,0:T(8,128)(2,1)}, bf16[128,4096]{1,0:T(8,128)(2,1)}, bf16[128,4096]{1,0:T(8,128)(2,1)}, bf16[2048,256]{1,0:T(8,128)(2,1)}, bf1...) custom-call(bf16[128,256]{1,0:T(8,128)(2,1)} %get-tuple-element.21.refs_0_, ...), custom_call_target="tpu_custom_call" | custom-call | tf_op jit(solution)/shard_map/pallas_call | solution.py:746

commit v4 on v3

--- a/solution.py
+++ b/solution.py
@@ -145,79 +145,6 @@
 
     idt[f] = jnp.concatenate([ids_ref[...].astype(F32), jnp.zeros((16 - K, TOK), F32)], axis=0).astype(BF16)
 
-    pl.semaphore_wait(bar, 2 * NF - 1 + NZ - 1)
-
-    def remote(src, dst, s, r, **where):
-        return pltpu.make_async_remote_copy(
-            src_ref=src, dst_ref=dst, send_sem=s, recv_sem=r,
-            device_id=where, device_id_type=pl.DeviceIdType.MESH,
-        )
-
-    steps = [i for d in range(1, NZ // 2 + 1) for i in dict.fromkeys((d, NZ - d))]
-
-    def along_z(src, stage, s, r):
-        for i in steps:
-            remote(src, stage.at[z], s.at[i], r.at[z], tp=((z + i) % NZ) * 2 + c).start()
-
-    def in_plane(src, stage, got, zs, zr, s, r, beside=None):
-        for n, i in enumerate([0] + [(NZ - i) for i in steps]):
-            zz = (z + i) % NZ
-            if i:
-                remote(src, stage.at[zz], zs.at[i], zr.at[zz], tp=zz * 2 + c).wait_recv()
-            part = stage.at[zz] if i else src
-            to = zz * 2 + c
-
-            @pl.when(to == f)
-            def _():
-                got[f] = part[...]
-
-            @pl.when(to != f)
-            def _():
-                remote(part, got.at[f], s.at[i], r.at[f], fs=to, tp=z * 2 + f % 2).start()
-
-            if beside is not None:
-                beside(n)
-
-    def wait_spread_sends(src, stage, got, zs, zr, s, r):
-        for i in range(NZ):
-            zz = (z + i) % NZ
-            to = zz * 2 + c
-            if i:
-                remote(src, stage.at[z], zs.at[i], zr.at[z], tp=zz * 2 + c).wait_send()
-
-            @pl.when(to != f)
-            def _():
-                remote(src, got.at[f], s.at[i], r.at[f], fs=to, tp=z * 2 + f % 2).wait_send()
-
-    def direct_block(i):
-        return 2 * ((f // 2 + i) % (NF // 2)) + c
-
-    def take_direct(b, got, s, r, ms, mr):
-        @pl.when(b != f)
-        def _():
-            remote(got.at[b], got.at[b], s.at[0], r.at[b], fs=b).wait_recv()
-
-        remote(got.at[b], got.at[b], ms.at[b], mr.at[b], tp=z * 2 + 1 - c).start()
-
-    def take_mate(b, got, ms, mr):
-        remote(got.at[b], got.at[b], ms.at[b], mr.at[b], tp=z * 2 + 1 - c).wait_recv()
-
-    def wait_mate_sends(got, ms, mr):
-        def body(i, carry):
-            b = direct_block(i)
-            remote(got.at[b], got.at[b], ms.at[b], mr.at[b], tp=z * 2 + 1 - c).wait_send()
-            return carry
-
-        lax.fori_loop(0, NF // 2, body, 0)
-
-    along_z(tok_ref, xz, xzs, xzr)
-
-    def send_ids(i, carry):
-        remote(idt.at[f], idt.at[f], ids_s.at[i], ids_r.at[f], fs=(f + i) % NF).start()
-        return carry
-
-    lax.fori_loop(1, NF, send_ids, 0)
-
     sr = lax.broadcasted_iota(jnp.int32, (16, K * LANES), 0)
     sc = lax.broadcasted_iota(jnp.int32, (16, K * LANES), 1)
     spread_ids[:, : K * LANES] = (sr == sc // LANES).astype(BF16)
@@ -243,6 +170,79 @@
     ws[0:HS, :DS] = (sgt_ref[...] * gain).astype(BF16)
     ws[HS : 2 * HS, :DS] = (sut_ref[...] * gain).astype(BF16)
     ws[2 * HS :, DS:] = ws[0 : 2 * HS, :DS]
+    pl.semaphore_wait(bar, 2 * NF - 1 + NZ - 1)
+
+    def remote(src, dst, s, r, **where):
+        return pltpu.make_async_remote_copy(
+            src_ref=src, dst_ref=dst, send_sem=s, recv_sem=r,
+            device_id=where, device_id_type=pl.DeviceIdType.MESH,
+        )
+
+    steps = [i for d in range(1, NZ // 2 + 1) for i in dict.fromkeys((d, NZ - d))]
+
+    def along_z(src, stage, s, r):
+        for i in steps:
+            remote(src, stage.at[z], s.at[i], r.at[z], tp=((z + i) % NZ) * 2 + c).start()
+
+    def in_plane(src, stage, got, zs, zr, s, r, beside=None):
+        for n, i in enumerate([0] + [(NZ - i) for i in steps]):
+            zz = (z + i) % NZ
+            if i:
+                remote(src, stage.at[zz], zs.at[i], zr.at[zz], tp=zz * 2 + c).wait_recv()
+            part = stage.at[zz] if i else src
+            to = zz * 2 + c
+
+            @pl.when(to == f)
+            def _():
+                got[f] = part[...]
+
+            @pl.when(to != f)
+            def _():
+                remote(part, got.at[f], s.at[i], r.at[f], fs=to, tp=z * 2 + f % 2).start()
+
+            if beside is not None:
+                beside(n)
+
+    def wait_spread_sends(src, stage, got, zs, zr, s, r):
+        for i in range(NZ):
+            zz = (z + i) % NZ
+            to = zz * 2 + c
+            if i:
+                remote(src, stage.at[z], zs.at[i], zr.at[z], tp=zz * 2 + c).wait_send()
+
+            @pl.when(to != f)
+            def _():
+                remote(src, got.at[f], s.at[i], r.at[f], fs=to, tp=z * 2 + f % 2).wait_send()
+
+    def direct_block(i):
+        return 2 * ((f // 2 + i) % (NF // 2)) + c
+
+    def take_direct(b, got, s, r, ms, mr):
+        @pl.when(b != f)
+        def _():
+            remote(got.at[b], got.at[b], s.at[0], r.at[b], fs=b).wait_recv()
+
+        remote(got.at[b], got.at[b], ms.at[b], mr.at[b], tp=z * 2 + 1 - c).start()
+
+    def take_mate(b, got, ms, mr):
+        remote(got.at[b], got.at[b], ms.at[b], mr.at[b], tp=z * 2 + 1 - c).wait_recv()
+
+    def wait_mate_sends(got, ms, mr):
+        def body(i, carry):
+            b = direct_block(i)
+            remote(got.at[b], got.at[b], ms.at[b], mr.at[b], tp=z * 2 + 1 - c).wait_send()
+            return carry
+
+        lax.fori_loop(0, NF // 2, body, 0)
+
+    along_z(tok_ref, xz, xzs, xzr)
+
+    def send_ids(i, carry):
+        remote(idt.at[f], idt.at[f], ids_s.at[i], ids_r.at[f], fs=(f + i) % NF).start()
+        return carry
+
+    lax.fori_loop(1, NF, send_ids, 0)
+
     for load in loads[:4]:
         load.wait()
     halves = [slice(q * LANES, (q + 1) * LANES) for q in range(DS // LANES)]

time: 126 us -> 126 us (level)
  no operation moved by 1% of the time
where the time goes in v4:
time: 126 us; the launch traced here: 123 us
  Pallas kernels  123 us (98%)
    pallas_call x1, Pallas kernels, body(): pl.pallas_call(functools.partial(kernel, NF, NT, D), out_shape=(jax.Shape...  119 us
    pallas_call x1, Pallas kernels, body(): pl.pallas_call(functools.partial(place, n), out_shape=shapes, in_specs=[h...  3.88 us

profile of v4, /device:TPU:42, one launch (start us, length us, event | category | flops | bytes accessed | tf_op | source)
XLA Modules:
  0.0 123.5 jit_solution(5977148834264670815)
XLA Ops:
  0.6 118.9 %shard_map.153 = (bf16[128,256]{1,0:T(8,128)(2,1)}, bf16[128,4096]{1,0:T(8,128)(2,1)}, bf16[128,4096]{1,0:T(8,128)(2,1)}, bf16[4,512,256]{2,1,0:T(8,128)(2,1)}, ...) custom-call(bf16[128,256]{1,0:T(8,128)(2,1)} %tok_ref.1, s32[8,128]{1,0:T(8,128)} %bitcast.14, ...), custom_call_target="tpu_custom_call" | custom-call | tf_op jit(solution)/shard_map/pallas_call | solution.py:679
  119.6 3.9 %shard_map.154 = (bf16[128,256]{1,0:T(8,128)(2,1)}, bf16[128,4096]{1,0:T(8,128)(2,1)}, bf16[128,4096]{1,0:T(8,128)(2,1)}, bf16[2048,256]{1,0:T(8,128)(2,1)}, bf1...) custom-call(bf16[128,256]{1,0:T(8,128)(2,1)} %get-tuple-element.21.refs_0_, ...), custom_call_target="tpu_custom_call" | custom-call | tf_op jit(solution)/shard_map/pallas_call | solution.py:746
